TPU v7x, 32 devices: a whole 2x2x4 slice. The times are simulated.
32 devices in a mesh: grp: 2 (over x), fs: 4 (over z), tp: 4 (over y, core).
Axes of the slice: x: 2, y: 2, z: 4, core: 2. Of those that a mesh axis runs over, the one named last changes fastest.
Arguments:
- tokens: bfloat16 [1024, 3584], P(('grp', 'fs')), parts along dimension 0, may hold values from -6 to 6
- norm_gain: float32 [3584], P('fs'), may hold values from 0.1 to 1.9
- up_master: float32 [3584, 14336], P('fs', 'tp'), may hold values from -0.09375 to 0.09375
- down_master: float32 [3584, 14336], P('fs', 'tp'), may hold values from -0.046875 to 0.046875
Outputs:
- up_ready: bfloat16 [7168, 14336], P('grp', 'tp'), parts along dimension 0
- down_ready: bfloat16 [7168, 14336], P('grp', 'tp'), parts along dimension 0
- mixed_out: bfloat16 [1024, 3584], P(('grp', 'fs', 'tp')), parts along dimension 0
There are 2 independent parts, one for each index of `grp`. A program takes and returns all parts, laid end to end along the dimension named above; an argument that names none is the same for every part. Nothing has to cross between parts.
All inputs are finite; a program needn't handle non-finite values.
Results may differ from a plain program's by a relative error of at most 0.024.
Values may be sent and summed in bfloat16 or wider, within the bound.
A program may use at most 192 MiB of HBM per device.

v0:
```python
import functools

import jax
import jax.numpy as jnp
from jax import lax
from jax.experimental import pallas as pl
from jax.experimental.pallas import tpu as pltpu
from jax.sharding import PartitionSpec as P

MESH = pl.DeviceIdType.MESH
VMEM_LIMIT = 60 * 1024 * 1024
ROWS = 512


def chunk_rows(half, width):
    for rows in range(16, half + 1, 16):
        if half % rows == 0 and rows * width * 2 >= 200 * 1024:
            return rows
    return half


def gather_kernel(sizes, gain, up, down, out, wide, narrow, load, store, zs, zr, own_s, xs, xr):
    groups, n, local, rows, count = sizes
    half = local // groups
    per = 2 * count
    g, f, t = lax.axis_index("grp"), lax.axis_index("fs"), lax.axis_index("tp")
    last = n - 1

    def loads(j, m):
        part = lax.rem(g + j, groups)
        master = (up, down)[m]

        def start(i, _):
            q = j * per + m * count + i
            first = pl.multiple_of(part * half + i * rows, 16)
            pltpu.make_async_copy(master.at[pl.ds(first, rows)], wide.at[q], load.at[q]).start()
            return _

        lax.fori_loop(0, count, start, 0)

    for j in range(groups):
        for m in range(2):
            loads(j, m)

    def where(source, part, q):
        m, i = q // count, q % count
        first = pl.multiple_of(source * local + part * half + i * rows, 16)
        return out.at[m, pl.ds(first, rows)]

    def convert(j, q):
        slot = j * per + q
        part = lax.rem(g + j, groups)
        pltpu.make_async_copy(up.at[pl.ds(0, rows)], wide.at[slot], load.at[slot]).wait()

        @pl.when(q < count)
        def _():
            first = pl.multiple_of(part * half + q * rows, 16)
            narrow[slot] = (gain[pl.ds(first, rows)] * wide[slot]).astype(jnp.bfloat16)

        @pl.when(q >= count)
        def _():
            narrow[slot] = wide[slot].astype(jnp.bfloat16)

    def keep(j, q):
        slot = j * per + q
        part = lax.rem(g + j, groups)
        return pltpu.make_async_copy(narrow.at[slot], where(f, part, q), store.at[slot])

    def own(way, q):
        to = f + 1 if way == 0 else f - 1
        return pltpu.make_async_remote_copy(
            narrow.at[q], where(f, g, q), own_s.at[way * per + q], zr.at[way * last * per + q],
            device_id=(g, to, t), device_id_type=MESH)

    def relay(way, k, q):
        source = f - k if way == 0 else f + k
        to = f + 1 if way == 0 else f - 1
        place = where(source, g, q)
        return pltpu.make_async_remote_copy(
            place, place, zs.at[(way * last + k - 1) * per + q], zr.at[(way * last + k) * per + q],
            device_id=(g, to, t), device_id_type=MESH)

    def arrival(way, k, q):
        source = f - k if way == 0 else f + k
        place = where(source, g, q)
        return pltpu.make_async_remote_copy(
            place, place, zs.at[0], zr.at[(way * last + k - 1) * per + q],
            device_id=(g, f, t), device_id_type=MESH)

    def across(j, way, k, q, part):
        source = f - k if way == 0 else f + k
        place = where(source, part, q)
        s = ((j * 2 + way) * last + k - 1) * per + q
        return pltpu.make_async_remote_copy(
            place, place, xs.at[s], xr.at[s],
            device_id=(lax.rem(g + 1 + j, groups), f, t), device_id_type=MESH)

    has = (f < last, f > 0)
    barrier = pltpu.get_barrier_semaphore()
    for way in range(2):
        @pl.when(has[way])
        def _(way=way):
            to = f + 1 if way == 0 else f - 1
            pl.semaphore_signal(barrier, inc=1, device_id=(g, to, t), device_id_type=MESH)
    for j in range(groups - 1):
        pl.semaphore_signal(barrier, inc=1, device_id=(lax.rem(g + 1 + j, groups), f, t), device_id_type=MESH)
    pl.semaphore_wait(barrier, groups - 1 + jnp.minimum(f, 1) + jnp.minimum(last - f, 1))

    def send_own(q):
        for way in range(2):
            @pl.when(has[way])
            def _(way=way):
                own(way, q).start()
        keep(0, q).start()

    def first_step(q, carry):
        convert(0, q)

        @pl.when(q > 0)
        def _():
            send_own(q - 1)
        return carry

    lax.fori_loop(0, per, first_step, 0)
    if groups > 1:
        convert(1, 0)
    send_own(per - 1)

    def step(k, q):
        for way in range(2):
            reach = (k <= f) if way == 0 else (k <= last - f)

            @pl.when(reach)
            def _(way=way):
                arrival(way, k, q).wait_recv()

                @pl.when(has[way])
                def _():
                    relay(way, k, q).start()
                for j in range(groups - 1):
                    across(j, way, k, q, g).start()

    def first_round(q, carry):
        step(1, q)
        for j in range(1, groups):
            if j > 1:
                convert(j, q)

            @pl.when(q + 1 < per)
            def _():
                if j == 1:
                    convert(1, q + 1)
            keep(j, q).start()
        return carry

    lax.fori_loop(0, per, first_round, 0)

    def later(r, carry):
        step(2 + r // per, r % per)
        return carry

    lax.fori_loop(0, (last - 1) * per, later, 0)

    def finish(r, carry):
        k, q = 1 + r // per, r % per
        for way in range(2):
            reach = (k <= f) if way == 0 else (k <= last - f)

            @pl.when(reach)
            def _(way=way):
                @pl.when(has[way])
                def _():
                    relay(way, k, q).wait_send()
                for j in range(groups - 1):
                    sender = lax.rem(g + groups - 1 - j, groups)
                    across(j, way, k, q, g).wait_send()
                    across(j, way, k, q, sender).wait_recv()
        return carry

    def finish_own(q, carry):
        for j in range(groups):
            keep(j, q).wait()
        for way in range(2):
            @pl.when(has[way])
            def _(way=way):
                own(way, q).wait_send()
        return carry

    lax.fori_loop(0, per, finish_own, 0)
    lax.fori_loop(0, last * per, finish, 0)


def gather(groups, n, gain, up, down):
    local, width = up.shape
    half = local // groups
    rows = chunk_rows(half, width)
    count = half // rows
    per = 2 * count
    last = n - 1
    dma = pltpu.SemaphoreType.DMA
    sent = 2 * (n - 1) * local * width * 2
    return pl.pallas_call(
        functools.partial(gather_kernel, (groups, n, local, rows, count)),
        out_shape=jax.ShapeDtypeStruct((2, n * local, width), jnp.bfloat16),
        in_specs=[pl.BlockSpec(memory_space=pltpu.VMEM)] + [pl.BlockSpec(memory_space=pl.ANY)] * 2,
        out_specs=pl.BlockSpec(memory_space=pl.ANY),
        scratch_shapes=[
            pltpu.VMEM((groups * per, rows, width), jnp.float32),
            pltpu.VMEM((groups * per, rows, width), jnp.bfloat16),
            dma((groups * per,)),
            dma((groups * per,)),
            dma((2 * last * per,)),
            dma((2 * last * per,)),
            dma((2 * per,)),
            dma((max(1, groups - 1) * 2 * last * per,)),
            dma((max(1, groups - 1) * 2 * last * per,)),
        ],
        compiler_params=pltpu.CompilerParams(
            collective_id=0, has_side_effects=True, vmem_limit_bytes=VMEM_LIMIT),
        cost_estimate=pl.CostEstimate(flops=0, bytes_accessed=sent, transcendentals=0),
        name="gather_both",
    )(gain[:, None], up, down)


def pass_kernel(steps, tokens, block, up_ready, down_ready, mixed, normed, total, hidden):
    step = pl.program_id(0)
    rows = block.shape[1]

    @pl.when(step == 0)
    def _():
        values = tokens[...].astype(jnp.float32)
        square_mean = jnp.mean(values * values, axis=1, keepdims=True)
        scaled = (values * lax.rsqrt(square_mean + 1e-06)).astype(jnp.bfloat16)
        for i in range(steps):
            normed[i] = scaled[:, i * rows:(i + 1) * rows]
        total[...] = jnp.zeros_like(total)

    @pl.when(step < steps)
    def _():
        weights = block[0]
        up_ready[...] = weights
        total[...] += jnp.dot(normed[step], weights, preferred_element_type=jnp.float32)

    @pl.when(step == steps - 1)
    def _():
        hidden[...] = jnp.square(jnp.maximum(total[...], 0.0)).astype(jnp.bfloat16)

    @pl.when(step >= steps)
    def _():
        weights = block[0]
        down_ready[...] = weights
        mixed[...] = lax.dot_general(
            hidden[...], weights, (((1,), (1,)), ((), ())), preferred_element_type=jnp.float32
        ).astype(jnp.bfloat16)


def sum_kernel(chips, part, out, pair, near, far, send, recv):
    g, f, t = lax.axis_index("grp"), lax.axis_index("fs"), lax.axis_index("tp")
    y, c = t // 2, lax.rem(t, 2)
    sibling = (g, f, 2 * y + 1 - c)

    def other(j):
        return lax.rem(y + j, chips)

    barrier = pltpu.get_barrier_semaphore()
    pl.semaphore_signal(barrier, inc=1, device_id=sibling, device_id_type=MESH)
    for j in range(1, chips):
        pl.semaphore_signal(barrier, inc=1, device_id=(g, f, 2 * other(j) + c), device_id_type=MESH)
    pl.semaphore_wait(barrier, chips)
    over, back = [], []
    for j in list(range(1, chips)) + [0]:
        copy = pltpu.make_async_remote_copy(
            part.at[2 * other(j) + 1 - c], near.at[j], send.at[j], recv.at[j],
            device_id=sibling, device_id_type=MESH)
        copy.start()
        over.append((j, copy))
    for j, copy in over:
        copy.wait_recv()
        both = part[2 * other(j) + c].astype(jnp.float32) + near[j].astype(jnp.float32)
        if j == 0:
            total = both
        else:
            pair[j] = both.astype(jnp.bfloat16)
            copy = pltpu.make_async_remote_copy(
                pair.at[j], far.at[j], send.at[chips + j], recv.at[chips + j],
                device_id=(g, f, 2 * other(j) + c), device_id_type=MESH)
            copy.start()
            back.append((j, copy))
    for j, copy in back:
        copy.wait_recv()
        total = total + far[j].astype(jnp.float32)
    out[...] = total.astype(jnp.bfloat16)
    for _, copy in over + back:
        copy.wait_send()


def per_device(groups, n, tp, tokens, norm_gain, up_master, down_master):
    both = gather(groups, n, norm_gain, up_master, down_master)
    depth, width = both.shape[1:]
    count = tokens.shape[0]
    rows = next(size for size in (ROWS, 256, 128, depth) if depth % size == 0)
    steps = depth // rows
    weight = jax.ShapeDtypeStruct((depth, width), jnp.bfloat16)
    up_ready, down_ready, mixed = pl.pallas_call(
        functools.partial(pass_kernel, steps),
        grid=(2 * steps,),
        in_specs=[
            pl.BlockSpec((count, depth), lambda i: (0, 0)),
            pl.BlockSpec((1, rows, width), lambda i: (i // steps, i % steps, 0)),
        ],
        out_specs=[
            pl.BlockSpec((rows, width), lambda i: (jnp.minimum(i, steps - 1), 0)),
            pl.BlockSpec((rows, width), lambda i: (jnp.maximum(i - steps, 0), 0)),
            pl.BlockSpec((count, rows), lambda i: (0, jnp.maximum(i - steps, 0))),
        ],
        out_shape=[weight, weight, jax.ShapeDtypeStruct((count, depth), jnp.bfloat16)],
        scratch_shapes=[
            pltpu.VMEM((steps, count, rows), jnp.bfloat16),
            pltpu.VMEM((count, width), jnp.float32),
            pltpu.VMEM((count, width), jnp.bfloat16),
        ],
        compiler_params=pltpu.CompilerParams(vmem_limit_bytes=VMEM_LIMIT),
        name="both_passes",
    )(tokens, both)
    share = count // tp
    chips = tp // 2
    held = pltpu.VMEM((chips, share, depth), jnp.bfloat16)
    mixed_out = pl.pallas_call(
        functools.partial(sum_kernel, chips),
        out_shape=jax.ShapeDtypeStruct((share, depth), jnp.bfloat16),
        in_specs=[pl.BlockSpec(memory_space=pltpu.VMEM)],
        out_specs=pl.BlockSpec(memory_space=pltpu.VMEM),
        scratch_shapes=[held, held, held] + [pltpu.SemaphoreType.DMA((2 * chips,))] * 2,
        compiler_params=pltpu.CompilerParams(
            collective_id=1, has_side_effects=True, vmem_limit_bytes=VMEM_LIMIT),
        name="sum_shares",
    )(mixed.reshape(tp, share, depth))
    return (up_ready, down_ready, mixed_out)


def solution(mesh):
    groups, n, tp = (mesh.shape[name] for name in ("grp", "fs", "tp"))
    return jax.shard_map(
        functools.partial(per_device, groups, n, tp),
        mesh=mesh,
        in_specs=(P(("grp", "fs"), None), P("fs"), P("fs", "tp"), P("fs", "tp")),
        out_specs=(P("grp", "tp"), P("grp", "tp"), P(("grp", "fs", "tp"), None)),
        check_vma=False,
    )
```

profile of v0, /device:TPU:0, one launch (start us, length us, event | category | flops | bytes accessed | tf_op | source)
XLA Modules:
  0.0 492.2 jit_solution(4575094930089935217)
XLA Ops:
  0.6 1.6 broadcast_in_dim.4.gain
  2.3 434.1 %gather_both.1.block = bf16[2,3584,3584]{2,1,0:T(8,128)(2,1)} custom-call(f32[896,1]{1,0:T(8,128)} %broadcast_in_dim.4.gain, f32[896,3584]{1,0:T(8,128)} %up.1, f32[896,3584]{1,0:T(8,128)} %down.1), custom_call_target="tpu_custom_call" | custom-call | bytes 38535168 | tf_op jit(solution)/shard_map/gather_both/pallas_call | solution.py:202
  436.4 42.9 %both_passes.1 = (bf16[3584,3584]{1,0:T(8,128)(2,1)}, bf16[3584,3584]{1,0:T(8,128)(2,1)}, bf16[128,3584]{1,0:T(8,128)(2,1)}) custom-call(bf16[128,3584]{1,0:T(8,128)(2,1)} %tokens.1, bf16[2,3584,3584]{2,1,0:T(8,128)(2,1)} %gather_both.1.block), custom_call_target="tpu_custom_call" | custom-call | tf_op jit(solution)/shard_map/both_passes/pallas_call | solution.py:304
  479.3 11.3 %sum_shares.1 = bf16[32,3584]{1,0:T(8,128)(2,1)} custom-call(bf16[4,32,3584]{2,1,0:T(8,128)(2,1)} %bitcast.1), custom_call_target="tpu_custom_call" | custom-call | tf_op jit(solution)/shard_map/sum_shares/pallas_call | solution.py:328
  490.6 1.6 copy.9
where the time goes:
time: 493 us; the launch traced here: 492 us
  Pallas kernels  488 us (99%)
    pallas_call x1, Pallas kernels, gather(): pl.pallas_call(functools.partial(gather_kernel, (groups, n, local, rows,...  434 us
    pallas_call x1, Pallas kernels, per_device(): pl.pallas_call(functools.partial(pass_kernel, steps), grid=(2 * steps,),...  42.9 us
    pallas_call x1, Pallas kernels, per_device(): pl.pallas_call(functools.partial(sum_kernel, chips), out_shape=jax.ShapeD...  11.3 us

commit v1 on v0

v1 whole, which is shorter than its diff:
```python
import functools

import jax
import jax.numpy as jnp
from jax import lax
from jax.experimental import pallas as pl
from jax.experimental.pallas import tpu as pltpu
from jax.sharding import PartitionSpec as P

MESH = pl.DeviceIdType.MESH
SLOTS = 12
LAG = 3


def divisor(total, most, least):
    for size in range(most, 0, -least):
        if total % size == 0:
            return size
    return total


def chunk_rows(block, width):
    for rows in range(16, block + 1, 16):
        if block % rows == 0 and rows * width * 2 >= 100 * 1024:
            return rows
    return block


def gather_kernel(sizes, tokens, gain, up, down, both, part, wide, column, held, normed, acc, hidden, load, token_s, zs, zr, xs, xr):
    n, local, block, rows, piece = sizes
    half = local // 2
    count = half // rows
    per_block = block // rows
    blocks = half // block
    last = n - 1
    span = last * count
    total = 2 * span
    slots = wide.shape[0]
    g, f, t = lax.axis_index("grp"), lax.axis_index("fs"), lax.axis_index("tp")
    other = 1 - g
    pieces = acc.shape[0]
    double = jnp.minimum(f, last - f)

    def start_load(m, which, q, index):
        first = pl.multiple_of(which * half + q * rows, 16)
        slot = lax.rem(index, slots)
        pltpu.make_async_copy((up, down)[m].at[pl.ds(first, rows)], wide.at[slot], load.at[slot]).start()

    def next_load(index):
        @pl.when(index < count)
        def _():
            start_load(0, g, index, index)

        for m in range(2):
            @pl.when((index >= count) & (index < 3 * count) & (lax.rem(index + count, 2) == m))
            def _(m=m):
                start_load(m, other, lax.div(index - count, 2), index)

        @pl.when((index >= 3 * count) & (index < 4 * count))
        def _():
            start_load(1, g, index - 3 * count, index)

    def where(m, source, which, q):
        first = pl.multiple_of(source * local + which * half + q * rows, 16)
        return both.at[m, pl.ds(first, rows)]

    def convert(m, which, q, index):
        slot = lax.rem(index, slots)
        pltpu.make_async_copy(up.at[pl.ds(0, rows)], wide.at[slot], load.at[slot]).wait()
        near = pl.multiple_of(which * half + q * rows, 16)
        first = pl.multiple_of(f * local + which * half + q * rows, 16)
        values = wide[slot]
        if m == 0:
            values = column[pl.ds(near, rows)] * values
        both[m, pl.ds(first, rows)] = values.astype(jnp.bfloat16)
        next_load(index + slots)

    has = (f < last, f > 0)

    def hop(way):
        return (g, f + 1 if way == 0 else f - 1, t)

    def origin(way, k):
        return f - k if way == 0 else f + k

    def reach(way, k):
        return (k <= f) if way == 0 else (k <= last - f)

    def z_at(way, m, k, q):
        return ((way * 2 + m) * last + k) * count + q

    def along(way, m, k, q):
        place = where(m, origin(way, k), g, q)
        return pltpu.make_async_remote_copy(
            place, place, zs.at[z_at(way, m, k, q)], zr.at[z_at(way, m, k, q)],
            device_id=hop(way), device_id_type=MESH)

    def arrival(way, m, k, q):
        place = where(m, origin(way, k), g, q)
        return pltpu.make_async_remote_copy(
            place, place, zs.at[0], zr.at[z_at(way, m, k - 1, q)],
            device_id=hop(way), device_id_type=MESH)

    def x_at(way, m, k, q):
        two = k <= double
        base = jnp.where(two, 2 * count * (k - 1), count * (k - 1 + double))
        return m * span + base + jnp.where(two, 2 * q + way, q)

    def x_of(i):
        m, j = lax.div(i, span), lax.rem(i, span)
        two = j < 2 * count * double
        single = jnp.maximum(j - 2 * count * double, 0)
        k = jnp.where(two, 1 + lax.div(j, 2 * count), 1 + double + lax.div(single, count))
        q = jnp.where(two, lax.div(lax.rem(j, 2 * count), 2), lax.rem(single, count))
        up_side = jnp.where(two, lax.rem(j, 2), jnp.where(f < last - f, 1, 0))
        source = f + (2 * up_side - 1) * k
        return m, source, q

    def across(m, source, which, q, i):
        place = where(m, source, which, q)
        return pltpu.make_async_remote_copy(
            place, place, xs.at[i], xr.at[i], device_id=(other, f, t), device_id_type=MESH)

    def send_own(m, q):
        for way in range(2):
            @pl.when(has[way])
            def _(way=way):
                along(way, m, 0, q).start()

    lax.fori_loop(0, slots, lambda i, c: (next_load(i), c)[1], 0)
    token_copy = pltpu.make_async_copy(tokens, held, token_s.at[0])
    token_copy.start()

    barrier = pltpu.get_barrier_semaphore()
    for way in range(2):
        @pl.when(has[way])
        def _(way=way):
            pl.semaphore_signal(barrier, inc=1, device_id=hop(way), device_id_type=MESH)
    pl.semaphore_signal(barrier, inc=1, device_id=(other, f, t), device_id_type=MESH)
    step_rows = divisor(local, 128, 8)
    eye = lax.broadcasted_iota(jnp.int32, (step_rows, step_rows), 0) == lax.broadcasted_iota(
        jnp.int32, (step_rows, step_rows), 1)
    for i in range(local // step_rows):
        line = gain[i:i + 1, :]
        column[i * step_rows:(i + 1) * step_rows, :] = jnp.sum(
            jnp.where(eye, line, 0.0), axis=1, keepdims=True)
    pl.semaphore_wait(barrier, 1 + jnp.minimum(f, 1) + jnp.minimum(last - f, 1))

    def first_step(q, carry):
        convert(0, g, q, q)

        @pl.when(q > 0)
        def _():
            send_own(0, q - 1)
        return carry

    lax.fori_loop(0, count, first_step, 0)
    token_copy.wait()
    values = held[...].astype(jnp.float32)
    square_mean = jnp.mean(values * values, axis=1, keepdims=True)
    send_own(0, count - 1)
    scaled = (values * lax.rsqrt(square_mean + 1e-06)).astype(jnp.bfloat16)
    for i in range(normed.shape[0]):
        normed[i] = scaled[:, i * block:(i + 1) * block]
    acc[...] = jnp.zeros_like(acc)

    def task(m, index):
        first = pl.multiple_of(index * block, 16)

        @pl.when(m == 0)
        def _():
            def body(p, carry):
                at = pl.multiple_of(p * piece, piece)
                acc[p] += jnp.dot(
                    normed[index], both[0, pl.ds(first, block), pl.ds(at, piece)],
                    preferred_element_type=jnp.float32)
                return carry
            lax.fori_loop(0, pieces, body, 0)

        @pl.when(m == 1)
        def _():
            def body(p, value):
                at = pl.multiple_of(p * piece, piece)
                return value + lax.dot_general(
                    hidden[p], both[1, pl.ds(first, block), pl.ds(at, piece)],
                    (((1,), (1,)), ((), ())), preferred_element_type=jnp.float32)
            value = lax.fori_loop(0, pieces, body, jnp.zeros((hidden.shape[1], block), jnp.float32))
            part[index] = value.astype(jnp.bfloat16)

    def forward(s):
        m, j = lax.div(s, span), lax.rem(s, span)
        k, q = 1 + lax.div(j, count), lax.rem(j, count)

        @pl.when(s < count)
        def _():
            for w in range(2):
                convert(w, other, s, count + 2 * s + w)

        @pl.when((s >= span - count) & (s < span))
        def _():
            convert(1, g, s - (span - count), 3 * count + s - (span - count))

        @pl.when((s > span - count) & (s <= span))
        def _():
            send_own(1, s - 1 - (span - count))

        for way in range(2):
            @pl.when(reach(way, k))
            def _(way=way):
                arrival(way, m, k, q).wait_recv()

                @pl.when(has[way])
                def _():
                    along(way, m, k, q).start()
                across(m, origin(way, k), g, q, x_at(way, m, k, q)).start()

    def absorb(i):
        m, j = lax.div(i, span), lax.rem(i, span)
        k, q = 1 + lax.div(j, count), lax.rem(j, count)
        _, source, xq = x_of(i)
        across(m, source, other, xq, i).wait_recv()
        every = 2 * blocks
        own = j - count

        def one(c, carry):
            z_full = lax.rem(q, per_block) == per_block - 1
            x_full = lax.rem(xq, per_block) == per_block - 1
            exists = jnp.where(
                c == 0, (k <= f) & z_full, jnp.where(
                    c == 1, (k <= last - f) & z_full, jnp.where(
                        c == 2, x_full, (own >= 0) & (own < every))))
            z_block = g * blocks + lax.div(q, per_block)
            index = jnp.where(
                c == 0, (f - k) * every + z_block, jnp.where(
                    c == 1, (f + k) * every + z_block, jnp.where(
                        c == 2, source * every + other * blocks + lax.div(xq, per_block),
                        f * every + own)))

            @pl.when(exists)
            def _():
                task(m, index)
            return carry

        lax.fori_loop(0, 4, one, 0)

        @pl.when(i == span - 1)
        def _():
            for p in range(pieces):
                hidden[p] = jnp.square(jnp.maximum(acc[p], 0.0)).astype(jnp.bfloat16)

    def step(s, carry):
        @pl.when(s < total)
        def _():
            forward(s)

        @pl.when(s >= LAG)
        def _():
            absorb(s - LAG)
        return carry

    lax.fori_loop(0, total + LAG, step, 0)

    def finish(s, carry):
        m, j = lax.div(s, span), lax.rem(s, span)
        k, q = lax.div(j, count), lax.rem(j, count)
        for way in range(2):
            @pl.when(has[way] & ((k == 0) | reach(way, k)))
            def _(way=way):
                along(way, m, k, q).wait_send()
        _, source, xq = x_of(s)
        across(m, source, g, xq, s).wait_send()
        return carry

    lax.fori_loop(0, total, finish, 0)


def gather(n, tokens, gain, up, down):
    local, width = up.shape
    count_rows = tokens.shape[0]
    half = local // 2
    block = divisor(half, 128, 16)
    rows = chunk_rows(block, width)
    count = half // rows
    depth = n * local
    piece = next(size for size in (512, 256, 128, width) if width % size == 0)
    moves = 2 * (n - 1) * count
    dma = pltpu.SemaphoreType.DMA
    step_rows = divisor(local, 128, 8)
    sent = 3 * (n - 1) * local * width * 2
    anywhere = pl.BlockSpec(memory_space=pl.ANY)
    inside = pl.BlockSpec(memory_space=pltpu.VMEM)
    return pl.pallas_call(
        functools.partial(gather_kernel, (n, local, block, rows, piece)),
        out_shape=[
            pltpu.VMEM((2, depth, width), jnp.bfloat16),
            pltpu.VMEM((depth // block, count_rows, block), jnp.bfloat16),
        ],
        in_specs=[anywhere, inside, anywhere, anywhere],
        out_specs=[inside, inside],
        scratch_shapes=[
            pltpu.VMEM((min(SLOTS, 4 * count), rows, width), jnp.float32),
            pltpu.VMEM((local, 1), jnp.float32),
            pltpu.VMEM((count_rows, depth), jnp.bfloat16),
            pltpu.VMEM((depth // block, count_rows, block), jnp.bfloat16),
            pltpu.VMEM((width // piece, count_rows, piece), jnp.float32),
            pltpu.VMEM((width // piece, count_rows, piece), jnp.bfloat16),
            dma((min(SLOTS, 4 * count),)),
            dma((1,)),
            dma((2 * moves,)),
            dma((2 * moves,)),
            dma((moves,)),
            dma((moves,)),
        ],
        compiler_params=pltpu.CompilerParams(
            collective_id=0, has_side_effects=True, vmem_limit_bytes=11 * 1024 * 1024),
        cost_estimate=pl.CostEstimate(flops=0, bytes_accessed=sent, transcendentals=0),
        name="gather_both",
    )(tokens, gain.reshape(local // step_rows, step_rows), up, down)


def sum_kernel(chips, part, out, pair, near, far, send, recv):
    g, f, t = lax.axis_index("grp"), lax.axis_index("fs"), lax.axis_index("tp")
    y, c = t // 2, lax.rem(t, 2)
    sibling = (g, f, 2 * y + 1 - c)

    def other(j):
        return lax.rem(y + j, chips)

    barrier = pltpu.get_barrier_semaphore()
    pl.semaphore_signal(barrier, inc=1, device_id=sibling, device_id_type=MESH)
    for j in range(1, chips):
        pl.semaphore_signal(barrier, inc=1, device_id=(g, f, 2 * other(j) + c), device_id_type=MESH)
    pl.semaphore_wait(barrier, chips)
    over, back = [], []
    for j in list(range(1, chips)) + [0]:
        copy = pltpu.make_async_remote_copy(
            part.at[2 * other(j) + 1 - c], near.at[j], send.at[j], recv.at[j],
            device_id=sibling, device_id_type=MESH)
        copy.start()
        over.append((j, copy))
    for j, copy in over:
        copy.wait_recv()
        both = part[2 * other(j) + c].astype(jnp.float32) + near[j].astype(jnp.float32)
        if j == 0:
            total = both
        else:
            pair[j] = both.astype(jnp.bfloat16)
            copy = pltpu.make_async_remote_copy(
                pair.at[j], far.at[j], send.at[chips + j], recv.at[chips + j],
                device_id=(g, f, 2 * other(j) + c), device_id_type=MESH)
            copy.start()
            back.append((j, copy))
    for j, copy in back:
        copy.wait_recv()
        total = total + far[j].astype(jnp.float32)
    out[...] = total.astype(jnp.bfloat16)
    for _, copy in over + back:
        copy.wait_send()


def write_kernel(parts, both, mixed, up_ready, down_ready, mixed_out, done):
    depth = both.shape[1]
    size = depth // parts
    copies = [pltpu.make_async_copy(mixed, mixed_out, done.at[2 * parts])]
    for m, ready in enumerate((up_ready, down_ready)):
        for i in range(parts):
            place = pl.ds(i * size, size)
            copies.append(pltpu.make_async_copy(both.at[m, place], ready.at[place], done.at[m * parts + i]))
    for copy in copies:
        copy.start()
    for copy in copies:
        copy.wait()


def per_device(n, tp, tokens, norm_gain, up_master, down_master):
    both, part = gather(n, tokens, norm_gain, up_master, down_master)
    depth, width = both.shape[1:]
    count = tokens.shape[0]
    mixed = part.transpose(1, 0, 2).reshape(count, depth)
    share = count // tp
    chips = tp // 2
    held = pltpu.VMEM((chips, share, depth), jnp.bfloat16)
    mixed_sum = pl.pallas_call(
        functools.partial(sum_kernel, chips),
        out_shape=jax.ShapeDtypeStruct((share, depth), jnp.bfloat16),
        in_specs=[pl.BlockSpec(memory_space=pltpu.VMEM)],
        out_specs=pl.BlockSpec(memory_space=pltpu.VMEM),
        scratch_shapes=[held, held, held] + [pltpu.SemaphoreType.DMA((2 * chips,))] * 2,
        compiler_params=pltpu.CompilerParams(
            collective_id=1, has_side_effects=True, vmem_limit_bytes=8 * 1024 * 1024),
        name="sum_shares",
    )(mixed.reshape(tp, share, depth))
    weight = jax.ShapeDtypeStruct((depth, width), jnp.bfloat16)
    anywhere = pl.BlockSpec(memory_space=pl.ANY)
    parts = 8
    return tuple(pl.pallas_call(
        functools.partial(write_kernel, parts),
        out_shape=[weight, weight, jax.ShapeDtypeStruct((share, depth), jnp.bfloat16)],
        in_specs=[anywhere, anywhere],
        out_specs=[anywhere] * 3,
        scratch_shapes=[pltpu.SemaphoreType.DMA((2 * parts + 1,))],
        compiler_params=pltpu.CompilerParams(vmem_limit_bytes=1024 * 1024),
        name="write_out",
    )(both, mixed_sum))


def solution(mesh):
    n, tp = (mesh.shape[name] for name in ("fs", "tp"))
    return jax.shard_map(
        functools.partial(per_device, n, tp),
        mesh=mesh,
        in_specs=(P(("grp", "fs"), None), P("fs"), P("fs", "tp"), P("fs", "tp")),
        out_specs=(P("grp", "tp"), P("grp", "tp"), P(("grp", "fs", "tp"), None)),
        check_vma=False,
    )
```

time: 493 us -> 504 us (1.022)
  local copies, waits for them, and re-layouts: 3.28 us -> 35.5 us
  Pallas kernels: 488 us -> 468 us
    unnamed x1 -> x4, local copies, waits for them, and re-layouts: 1.64 us -> 32.6 us
    pallas_call x2, Pallas kernels: 477 us -> 458 us  [the longest x1 442 us: gather(): pl.pallas_call(functools.partial(gather_kernel, (n, local, block, rows, p...]
where the time goes in v1:
time: 504 us
  Pallas kernels  468 us (93%)
  local copies, waits for them, and re-layouts  35.5 us (7%)
    pallas_call x1, Pallas kernels, gather(): pl.pallas_call(functools.partial(gather_kernel, (n, local, block, rows, p...  442 us
    unnamed x4, local copies, waits for them, and re-layouts  32.6 us
    pallas_call x1, Pallas kernels, per_device(): pl.pallas_call(functools.partial(write_kernel, parts), out_shape=[weight,...  16.6 us

profile of v1, /device:TPU:0, one launch (start us, length us, event | category | flops | bytes accessed | tf_op | source)
XLA Modules:
  0.0 504.0 jit_solution(11903326420730694646)
XLA Ops:
  0.6 441.7 %gather_both.1 = (bf16[2,3584,3584]{2,1,0:T(8,128)(2,1)S(1)}, bf16[32,128,112]{2,1,0:T(8,128)(2,1)S(1)}) custom-call(bf16[128,3584]{1,0:T(8,128)(2,1)} %tokens.1, f32[7,128]{1,0:T(8,128)} %bitcast.3, f32[896,3584]{1,0:T(8,128)} %up.1, f32[896,3584]{1,0:T(8,128)} %down.1), custom_call_target="tpu_custom_call" | custom-call | bytes 57802752 | tf_op jit(solution)/shard_map/gather_both/pallas_call | solution.py:292
  442.3 0.0 copy-start
  442.3 16.9 %copy-done = bf16[2,3584,3584]{2,1,0:T(8,128)(2,1)} copy-done((bf16[2,3584,3584]{2,1,0:T(8,128)(2,1)}, bf16[2,3584,3584]{2,1,0:T(8,128)(2,1)S(1)}, u32[]{:S(2)}) %copy-start) | copy-done | bytes 51380248
  459.2 0.7 copy.8
  459.9 2.2 reshape_reshape.3.part
  462.1 9.5 %sum_shares.1.mixed = bf16[32,3584]{1,0:T(8,128)(2,1)S(1)} custom-call(bf16[4,32,3584]{2,1,0:T(8,128)(2,1)S(1)} %reshape_reshape.3.part), custom_call_target="tpu_custom_call" | custom-call | tf_op jit(solution)/shard_map/sum_shares/pallas_call | solution.py:383
  471.6 0.0 copy-start.1
  471.7 15.7 %copy-done.1 = bf16[2,3584,3584]{2,1,0:T(8,128)(2,1)S(1)} copy-done((bf16[2,3584,3584]{2,1,0:T(8,128)(2,1)S(1)}, bf16[2,3584,3584]{2,1,0:T(8,128)(2,1)}, u32[]{:S(2)}) %copy-start.1) | copy-done | bytes 51380248
  487.4 16.6 %write_out.1 = (bf16[3584,3584]{1,0:T(8,128)(2,1)}, bf16[3584,3584]{1,0:T(8,128)(2,1)}, bf16[32,3584]{1,0:T(8,128)(2,1)}) custom-call(bf16[2,3584,3584]{2,1,0:T(8,128)(2,1)S(1)} %copy-done.1, bf16[32,3584]{1,0:T(8,128)(2,1)S(1)} %sum_shares.1.mixed), custom_call_target="tpu_custom_call" | custom-call | tf_op jit(solution)/shard_map/write_out/pallas_call | solution.py:396
Async XLA Ops:
  442.3 16.9 %copy-start = (bf16[2,3584,3584]{2,1,0:T(8,128)(2,1)}, bf16[2,3584,3584]{2,1,0:T(8,128)(2,1)S(1)}, u32[]{:S(2)}) copy-start(bf16[2,3584,3584]{2,1,0:T(8,128)(2,1)S(1)} %get-tuple-element.5.both) | copy-start | bytes 154140672
  471.6 15.7 %copy-start.1 = (bf16[2,3584,3584]{2,1,0:T(8,128)(2,1)S(1)}, bf16[2,3584,3584]{2,1,0:T(8,128)(2,1)}, u32[]{:S(2)}) copy-start(bf16[2,3584,3584]{2,1,0:T(8,128)(2,1)} %copy-done) | copy-start | bytes 154140672

commit v2 on v1

--- a/solution.py
+++ b/solution.py
@@ -9,7 +9,7 @@
 
 MESH = pl.DeviceIdType.MESH
 SLOTS = 12
-LAG = 3
+LAG = 5
 
 
 def divisor(total, most, least):
@@ -26,8 +26,9 @@
     return block
 
 
-def gather_kernel(sizes, tokens, gain, up, down, both, part, wide, column, held, normed, acc, hidden, load, token_s, zs, zr, xs, xr):
-    n, local, block, rows, piece = sizes
+def gather_kernel(sizes, tokens, gain, up, down, both, out, wide, column, held, normed, acc, hidden, product,
+                  part, near, pair, kept, far, load, token_s, zs, zr, xs, xr, ss, sr, bs, br):
+    n, tp, local, block, rows, piece = sizes
     half = local // 2
     count = half // rows
     per_block = block // rows
@@ -38,7 +39,12 @@
     slots = wide.shape[0]
     g, f, t = lax.axis_index("grp"), lax.axis_index("fs"), lax.axis_index("tp")
     other = 1 - g
+    chips = tp // 2
+    y, c = t // 2, lax.rem(t, 2)
+    every = 2 * blocks
+    share = kept.shape[1]
     pieces = acc.shape[0]
+    each = -(-pieces // per_block)
     double = jnp.minimum(f, last - f)
 
     def start_load(m, which, q, index):
@@ -137,6 +143,14 @@
         def _(way=way):
             pl.semaphore_signal(barrier, inc=1, device_id=hop(way), device_id_type=MESH)
     pl.semaphore_signal(barrier, inc=1, device_id=(other, f, t), device_id_type=MESH)
+    sibling = (g, f, 2 * y + 1 - c)
+    pl.semaphore_signal(barrier, inc=1, device_id=sibling, device_id_type=MESH)
+
+    def chip(j):
+        return lax.rem(y + j, chips)
+
+    for j in range(1, chips):
+        pl.semaphore_signal(barrier, inc=1, device_id=(g, f, 2 * chip(j) + c), device_id_type=MESH)
     step_rows = divisor(local, 128, 8)
     eye = lax.broadcasted_iota(jnp.int32, (step_rows, step_rows), 0) == lax.broadcasted_iota(
         jnp.int32, (step_rows, step_rows), 1)
@@ -144,7 +158,7 @@
         line = gain[i:i + 1, :]
         column[i * step_rows:(i + 1) * step_rows, :] = jnp.sum(
             jnp.where(eye, line, 0.0), axis=1, keepdims=True)
-    pl.semaphore_wait(barrier, 1 + jnp.minimum(f, 1) + jnp.minimum(last - f, 1))
+    pl.semaphore_wait(barrier, 1 + chips + jnp.minimum(f, 1) + jnp.minimum(last - f, 1))
 
     def first_step(q, carry):
         convert(0, g, q, q)
@@ -160,32 +174,106 @@
     square_mean = jnp.mean(values * values, axis=1, keepdims=True)
     send_own(0, count - 1)
     scaled = (values * lax.rsqrt(square_mean + 1e-06)).astype(jnp.bfloat16)
+    scaled = jnp.concatenate(
+        [scaled[i * share:(i + 1) * share] for i in list(range(0, tp, 2)) + list(range(1, tp, 2))])
     for i in range(normed.shape[0]):
         normed[i] = scaled[:, i * block:(i + 1) * block]
     acc[...] = jnp.zeros_like(acc)
 
-    def task(m, index):
+    def slot_of(period, slot):
+        i = period * per_block - 1
+        m, j = lax.div(i, span), lax.rem(i, span)
+        k, q = 1 + lax.div(j, count), lax.rem(j, count)
+        z_block = g * blocks + lax.div(q, per_block)
+        two = j < 2 * count * double
+        single = jnp.maximum(j - 2 * count * double, 0)
+        xk = jnp.where(two, 1 + lax.div(j, 2 * count), 1 + double + lax.div(single, count))
+        xq = jnp.where(two, lax.div(lax.rem(j, 2 * count), 2), lax.rem(single, count))
+        x_full = jnp.where(two, lax.rem(j, 2 * per_block) == 2 * per_block - 1, slot == 2)
+        above = jnp.where(two, slot == 3, f < last - f)
+        source = jnp.where(above, f + xk, f - xk)
+        own = lax.div(j - count, per_block)
+        exists = (period > 0) & jnp.where(
+            slot == 0, k <= f, jnp.where(
+                slot == 1, k <= last - f, jnp.where(
+                    slot == 4, (j >= count) & (own < every), x_full)))
+        index = jnp.where(
+            slot == 0, (f - k) * every + z_block, jnp.where(
+                slot == 1, (f + k) * every + z_block, jnp.where(
+                    slot == 4, f * every + own,
+                    source * every + other * blocks + lax.div(xq, per_block))))
+        return exists, m, index
+
+    def multiply(m, index, slot, p):
         first = pl.multiple_of(index * block, 16)
+        at = pl.multiple_of(p * piece, piece)
 
         @pl.when(m == 0)
         def _():
-            def body(p, carry):
-                at = pl.multiple_of(p * piece, piece)
-                acc[p] += jnp.dot(
-                    normed[index], both[0, pl.ds(first, block), pl.ds(at, piece)],
-                    preferred_element_type=jnp.float32)
-                return carry
-            lax.fori_loop(0, pieces, body, 0)
+            acc[p] += jnp.dot(
+                normed[index], both[0, pl.ds(first, block), pl.ds(at, piece)],
+                preferred_element_type=jnp.float32)
 
         @pl.when(m == 1)
         def _():
-            def body(p, value):
-                at = pl.multiple_of(p * piece, piece)
-                return value + lax.dot_general(
-                    hidden[p], both[1, pl.ds(first, block), pl.ds(at, piece)],
-                    (((1,), (1,)), ((), ())), preferred_element_type=jnp.float32)
-            value = lax.fori_loop(0, pieces, body, jnp.zeros((hidden.shape[1], block), jnp.float32))
-            part[index] = value.astype(jnp.bfloat16)
+            value = lax.dot_general(
+                hidden[p], both[1, pl.ds(first, block), pl.ds(at, piece)],
+                (((1,), (1,)), ((), ())), preferred_element_type=jnp.float32)
+
+            @pl.when(p == 0)
+            def _():
+                product[slot] = value
+
+            @pl.when(p > 0)
+            def _():
+                product[slot] += value
+
+    mine = pl.multiple_of(c * (chips * share), 4)
+    theirs = pl.multiple_of((1 - c) * (chips * share), 4)
+
+    def over(index):
+        return pltpu.make_async_remote_copy(
+            part.at[index, pl.ds(theirs, chips * share)], near.at[index], ss.at[index], sr.at[index],
+            device_id=sibling, device_id_type=MESH)
+
+    def back(index, j):
+        at = index * (chips - 1) + j - 1
+        return pltpu.make_async_remote_copy(
+            pair.at[index, chip(j)], far.at[index, j - 1], bs.at[at], br.at[at],
+            device_id=(g, f, 2 * chip(j) + c), device_id_type=MESH)
+
+    def stage(which, period):
+        def one(slot, carry):
+            exists, m, index = slot_of(period, slot)
+
+            @pl.when(exists & (m == 1))
+            def _():
+                if which == 0:
+                    part[index] = product[slot].astype(jnp.bfloat16)
+                elif which == 1:
+                    over(index).start()
+                elif which == 2:
+                    over(index).wait_recv()
+                    value = part[index, pl.ds(mine, chips * share)].astype(jnp.float32) + near[index].astype(jnp.float32)
+                    for j in range(chips):
+                        rows_j = value[j * share:(j + 1) * share]
+                        pair[index, j] = rows_j.astype(jnp.bfloat16)
+
+                        @pl.when(y == j)
+                        def _(rows_j=rows_j):
+                            kept[index] = rows_j
+                elif which == 3:
+                    for j in range(1, chips):
+                        back(index, j).start()
+                else:
+                    value = kept[index]
+                    for j in range(1, chips):
+                        back(index, j).wait_recv()
+                        value = value + far[index, j - 1].astype(jnp.float32)
+                    out[index] = value.astype(jnp.bfloat16)
+            return carry
+
+        lax.fori_loop(0, 5, one, 0)
 
     def forward(s):
         m, j = lax.div(s, span), lax.rem(s, span)
@@ -215,38 +303,38 @@
                 across(m, origin(way, k), g, q, x_at(way, m, k, q)).start()
 
     def absorb(i):
-        m, j = lax.div(i, span), lax.rem(i, span)
-        k, q = 1 + lax.div(j, count), lax.rem(j, count)
-        _, source, xq = x_of(i)
-        across(m, source, other, xq, i).wait_recv()
-        every = 2 * blocks
-        own = j - count
-
-        def one(c, carry):
-            z_full = lax.rem(q, per_block) == per_block - 1
-            x_full = lax.rem(xq, per_block) == per_block - 1
-            exists = jnp.where(
-                c == 0, (k <= f) & z_full, jnp.where(
-                    c == 1, (k <= last - f) & z_full, jnp.where(
-                        c == 2, x_full, (own >= 0) & (own < every))))
-            z_block = g * blocks + lax.div(q, per_block)
-            index = jnp.where(
-                c == 0, (f - k) * every + z_block, jnp.where(
-                    c == 1, (f + k) * every + z_block, jnp.where(
-                        c == 2, source * every + other * blocks + lax.div(xq, per_block),
-                        f * every + own)))
+        @pl.when(i < total)
+        def _():
+            _, source, xq = x_of(i)
+            across(0, source, other, xq, i).wait_recv()
+
+        period, p = lax.div(i, per_block), lax.rem(i, per_block)
+
+        def one(slot, carry):
+            exists, m, index = slot_of(period, slot)
 
             @pl.when(exists)
             def _():
-                task(m, index)
+                def body(r, carry):
+                    multiply(m, index, slot, r)
+                    return carry
+                lax.fori_loop(p * each, jnp.minimum((p + 1) * each, pieces), body, 0)
             return carry
 
-        lax.fori_loop(0, 4, one, 0)
-
-        @pl.when(i == span - 1)
-        def _():
-            for p in range(pieces):
-                hidden[p] = jnp.square(jnp.maximum(acc[p], 0.0)).astype(jnp.bfloat16)
+        lax.fori_loop(0, 5, one, 0)
+
+        @pl.when(p == per_block - 1)
+        def _():
+            stage(0, period)
+            stage(2, period - 1)
+            stage(1, period)
+            stage(3, period - 1)
+            stage(4, period - 2)
+
+        @pl.when(i == span + per_block - 1)
+        def _():
+            for r in range(pieces):
+                hidden[r] = jnp.square(jnp.maximum(acc[r], 0.0)).astype(jnp.bfloat16)
 
     def step(s, carry):
         @pl.when(s < total)
@@ -258,7 +346,12 @@
             absorb(s - LAG)
         return carry
 
-    lax.fori_loop(0, total + LAG, step, 0)
+    lax.fori_loop(0, total + LAG + per_block, step, 0)
+    final = total // per_block
+    stage(2, final)
+    stage(3, final)
+    stage(4, final - 1)
+    stage(4, final)
 
     def finish(s, carry):
         m, j = lax.div(s, span), lax.rem(s, span)
@@ -273,8 +366,16 @@
 
     lax.fori_loop(0, total, finish, 0)
 
-
-def gather(n, tokens, gain, up, down):
+    def finish_sum(index, carry):
+        over(index).wait_send()
+        for j in range(1, chips):
+            back(index, j).wait_send()
+        return carry
+
+    lax.fori_loop(0, n * every, finish_sum, 0)
+
+
+def gather(n, tp, tokens, gain, up, down):
     local, width = up.shape
     count_rows = tokens.shape[0]
     half = local // 2
@@ -284,16 +385,17 @@
     depth = n * local
     piece = next(size for size in (512, 256, 128, width) if width % size == 0)
     moves = 2 * (n - 1) * count
+    share, chips, total = count_rows // tp, tp // 2, depth // block
     dma = pltpu.SemaphoreType.DMA
     step_rows = divisor(local, 128, 8)
     sent = 3 * (n - 1) * local * width * 2
     anywhere = pl.BlockSpec(memory_space=pl.ANY)
     inside = pl.BlockSpec(memory_space=pltpu.VMEM)
     return pl.pallas_call(
-        functools.partial(gather_kernel, (n, local, block, rows, piece)),
+        functools.partial(gather_kernel, (n, tp, local, block, rows, piece)),
         out_shape=[
             pltpu.VMEM((2, depth, width), jnp.bfloat16),
-            pltpu.VMEM((depth // block, count_rows, block), jnp.bfloat16),
+            pltpu.VMEM((total, share, block), jnp.bfloat16),
         ],
         in_specs=[anywhere, inside, anywhere, anywhere],
         out_specs=[inside, inside],
@@ -304,104 +406,64 @@
             pltpu.VMEM((depth // block, count_rows, block), jnp.bfloat16),
             pltpu.VMEM((width // piece, count_rows, piece), jnp.float32),
             pltpu.VMEM((width // piece, count_rows, piece), jnp.bfloat16),
+            pltpu.VMEM((5, count_rows, block), jnp.float32),
+            pltpu.VMEM((total, count_rows, block), jnp.bfloat16),
+            pltpu.VMEM((total, count_rows // 2, block), jnp.bfloat16),
+            pltpu.VMEM((total, chips, share, block), jnp.bfloat16),
+            pltpu.VMEM((total, share, block), jnp.float32),
+            pltpu.VMEM((total, chips - 1, share, block), jnp.bfloat16),
             dma((min(SLOTS, 4 * count),)),
             dma((1,)),
             dma((2 * moves,)),
             dma((2 * moves,)),
             dma((moves,)),
             dma((moves,)),
+            dma((total,)),
+            dma((total,)),
+            dma((total * (chips - 1),)),
+            dma((total * (chips - 1),)),
         ],
         compiler_params=pltpu.CompilerParams(
-            collective_id=0, has_side_effects=True, vmem_limit_bytes=11 * 1024 * 1024),
+            collective_id=0, has_side_effects=True, vmem_limit_bytes=27 * 512 * 1024),
         cost_estimate=pl.CostEstimate(flops=0, bytes_accessed=sent, transcendentals=0),
         name="gather_both",
     )(tokens, gain.reshape(local // step_rows, step_rows), up, down)
 
 
-def sum_kernel(chips, part, out, pair, near, far, send, recv):
-    g, f, t = lax.axis_index("grp"), lax.axis_index("fs"), lax.axis_index("tp")
-    y, c = t // 2, lax.rem(t, 2)
-    sibling = (g, f, 2 * y + 1 - c)
-
-    def other(j):
-        return lax.rem(y + j, chips)
-
-    barrier = pltpu.get_barrier_semaphore()
-    pl.semaphore_signal(barrier, inc=1, device_id=sibling, device_id_type=MESH)
-    for j in range(1, chips):
-        pl.semaphore_signal(barrier, inc=1, device_id=(g, f, 2 * other(j) + c), device_id_type=MESH)
-    pl.semaphore_wait(barrier, chips)
-    over, back = [], []
-    for j in list(range(1, chips)) + [0]:
-        copy = pltpu.make_async_remote_copy(
-            part.at[2 * other(j) + 1 - c], near.at[j], send.at[j], recv.at[j],
-            device_id=sibling, device_id_type=MESH)
-        copy.start()
-        over.append((j, copy))
-    for j, copy in over:
-        copy.wait_recv()
-        both = part[2 * other(j) + c].astype(jnp.float32) + near[j].astype(jnp.float32)
-        if j == 0:
-            total = both
-        else:
-            pair[j] = both.astype(jnp.bfloat16)
-            copy = pltpu.make_async_remote_copy(
-                pair.at[j], far.at[j], send.at[chips + j], recv.at[chips + j],
-                device_id=(g, f, 2 * other(j) + c), device_id_type=MESH)
-            copy.start()
-            back.append((j, copy))
-    for j, copy in back:
-        copy.wait_recv()
-        total = total + far[j].astype(jnp.float32)
-    out[...] = total.astype(jnp.bfloat16)
-    for _, copy in over + back:
-        copy.wait_send()
-
-
 def write_kernel(parts, both, mixed, up_ready, down_ready, mixed_out, done):
     depth = both.shape[1]
     size = depth // parts
-    copies = [pltpu.make_async_copy(mixed, mixed_out, done.at[2 * parts])]
+    copies = []
     for m, ready in enumerate((up_ready, down_ready)):
         for i in range(parts):
             place = pl.ds(i * size, size)
             copies.append(pltpu.make_async_copy(both.at[m, place], ready.at[place], done.at[m * parts + i]))
     for copy in copies:
         copy.start()
+    block = mixed.shape[2]
+    for i in range(mixed.shape[0]):
+        mixed_out[:, i * block:(i + 1) * block] = mixed[i]
     for copy in copies:
         copy.wait()
 
 
 def per_device(n, tp, tokens, norm_gain, up_master, down_master):
-    both, part = gather(n, tokens, norm_gain, up_master, down_master)
+    both, mixed = gather(n, tp, tokens, norm_gain, up_master, down_master)
     depth, width = both.shape[1:]
-    count = tokens.shape[0]
-    mixed = part.transpose(1, 0, 2).reshape(count, depth)
-    share = count // tp
-    chips = tp // 2
-    held = pltpu.VMEM((chips, share, depth), jnp.bfloat16)
-    mixed_sum = pl.pallas_call(
-        functools.partial(sum_kernel, chips),
-        out_shape=jax.ShapeDtypeStruct((share, depth), jnp.bfloat16),
-        in_specs=[pl.BlockSpec(memory_space=pltpu.VMEM)],
-        out_specs=pl.BlockSpec(memory_space=pltpu.VMEM),
-        scratch_shapes=[held, held, held] + [pltpu.SemaphoreType.DMA((2 * chips,))] * 2,
-        compiler_params=pltpu.CompilerParams(
-            collective_id=1, has_side_effects=True, vmem_limit_bytes=8 * 1024 * 1024),
-        name="sum_shares",
-    )(mixed.reshape(tp, share, depth))
+    share = mixed.shape[1]
     weight = jax.ShapeDtypeStruct((depth, width), jnp.bfloat16)
     anywhere = pl.BlockSpec(memory_space=pl.ANY)
+    inside = pl.BlockSpec(memory_space=pltpu.VMEM)
     parts = 8
     return tuple(pl.pallas_call(
         functools.partial(write_kernel, parts),
         out_shape=[weight, weight, jax.ShapeDtypeStruct((share, depth), jnp.bfloat16)],
-        in_specs=[anywhere, anywhere],
-        out_specs=[anywhere] * 3,
-        scratch_shapes=[pltpu.SemaphoreType.DMA((2 * parts + 1,))],
-        compiler_params=pltpu.CompilerParams(vmem_limit_bytes=1024 * 1024),
+        in_specs=[anywhere, inside],
+        out_specs=[anywhere, anywhere, inside],
+        scratch_shapes=[pltpu.SemaphoreType.DMA((2 * parts,))],
+        compiler_params=pltpu.CompilerParams(vmem_limit_bytes=27 * 512 * 1024),
         name="write_out",
-    )(both, mixed_sum))
+    )(pltpu.with_memory_space_constraint(both, pltpu.VMEM), pltpu.with_memory_space_constraint(mixed, pltpu.VMEM)))
 
 
 def solution(mesh):

time: 504 us -> 471 us (0.935)
  local copies, waits for them, and re-layouts: 35.5 us -> 0 us
    unnamed x4 -> x0, local copies, waits for them, and re-layouts: 32.6 us -> none
    pallas_call x2 -> x1, Pallas kernels: 451 us -> 453 us  [gather(): pl.pallas_call(functools.partial(gather_kernel, (n, tp, local, block, row...]
where the time goes in v2:
time: 471 us
  Pallas kernels  470 us (100%)
    pallas_call x1, Pallas kernels, gather(): pl.pallas_call(functools.partial(gather_kernel, (n, tp, local, block, row...  453 us
    pallas_call x1, Pallas kernels, per_device(): pl.pallas_call(functools.partial(write_kernel, parts), out_shape=[weight,...  17.2 us

profile of v2, /device:TPU:0, one launch (start us, length us, event | category | flops | bytes accessed | tf_op | source)
XLA Modules:
  0.0 470.5 jit_solution(7955178775066063802)
XLA Ops:
  0.6 452.7 %gather_both.1 = (bf16[2,3584,3584]{2,1,0:T(8,128)(2,1)S(1)}, bf16[32,32,112]{2,1,0:T(8,128)(2,1)S(1)}) custom-call(bf16[128,3584]{1,0:T(8,128)(2,1)} %tokens.1, f32[7,128]{1,0:T(8,128)} %bitcast.1, f32[896,3584]{1,0:T(8,128)} %up.1, f32[896,3584]{1,0:T(8,128)} %down.1), custom_call_target="tpu_custom_call" | custom-call | bytes 57802752 | tf_op jit(solution)/shard_map/gather_both/pallas_call | solution.py:394
  453.3 17.2 %write_out.1 = (bf16[3584,3584]{1,0:T(8,128)(2,1)}, bf16[3584,3584]{1,0:T(8,128)(2,1)}, bf16[32,3584]{1,0:T(8,128)(2,1)}) custom-call(bf16[2,3584,3584]{2,1,0:T(8,128)(2,1)S(1)} %get-tuple-element.5.both, bf16[32,32,112]{2,1,0:T(8,128)(2,1)S(1)} %get-tuple-element.6.mixed), custom_call_target="tpu_custom_call" | custom-call | tf_op jit(solution)/shard_map/write_out/pallas_call | solution.py:458

commit v3 on v2

--- a/solution.py
+++ b/solution.py
@@ -8,8 +8,8 @@
 from jax.sharding import PartitionSpec as P
 
 MESH = pl.DeviceIdType.MESH
-SLOTS = 12
-LAG = 5
+SLOTS = 6
+LAG = 2
 
 
 def divisor(total, most, least):
@@ -21,7 +21,7 @@
 
 def chunk_rows(block, width):
     for rows in range(16, block + 1, 16):
-        if block % rows == 0 and rows * width * 2 >= 100 * 1024:
+        if block % rows == 0 and rows * width * 2 >= 200 * 1024:
             return rows
     return block
 
@@ -98,8 +98,15 @@
     def along(way, m, k, q):
         place = where(m, origin(way, k), g, q)
         return pltpu.make_async_remote_copy(
-            place, place, zs.at[z_at(way, m, k, q)], zr.at[z_at(way, m, k, q)],
+            place, place, zs.at[(way * 2 + m) * last + k], zr.at[z_at(way, m, k, q)],
             device_id=hop(way), device_id_type=MESH)
+
+    def all_rows(m, source, way, k, across_x):
+        place = both.at[m, pl.ds(pl.multiple_of(source * local + g * half, 16), half)]
+        at = (way * 2 + m) * last + k
+        return pltpu.make_async_remote_copy(
+            place, place, (xs if across_x else zs).at[at], zr.at[0],
+            device_id=(other, f, t) if across_x else hop(way), device_id_type=MESH)
 
     def arrival(way, m, k, q):
         place = where(m, origin(way, k), g, q)
@@ -122,10 +129,10 @@
         source = f + (2 * up_side - 1) * k
         return m, source, q
 
-    def across(m, source, which, q, i):
+    def across(m, source, which, q, sent, i):
         place = where(m, source, which, q)
         return pltpu.make_async_remote_copy(
-            place, place, xs.at[i], xr.at[i], device_id=(other, f, t), device_id_type=MESH)
+            place, place, xs.at[sent], xr.at[i], device_id=(other, f, t), device_id_type=MESH)
 
     def send_own(m, q):
         for way in range(2):
@@ -192,11 +199,11 @@
         x_full = jnp.where(two, lax.rem(j, 2 * per_block) == 2 * per_block - 1, slot == 2)
         above = jnp.where(two, slot == 3, f < last - f)
         source = jnp.where(above, f + xk, f - xk)
-        own = lax.div(j - count, per_block)
+        own = lax.div(j + 1 - count, per_block)
         exists = (period > 0) & jnp.where(
             slot == 0, k <= f, jnp.where(
                 slot == 1, k <= last - f, jnp.where(
-                    slot == 4, (j >= count) & (own < every), x_full)))
+                    slot == 4, (j + 1 >= count) & (own < every), x_full)))
         index = jnp.where(
             slot == 0, (f - k) * every + z_block, jnp.where(
                 slot == 1, (f + k) * every + z_block, jnp.where(
@@ -233,16 +240,16 @@
 
     def over(index):
         return pltpu.make_async_remote_copy(
-            part.at[index, pl.ds(theirs, chips * share)], near.at[index], ss.at[index], sr.at[index],
+            part.at[index, pl.ds(theirs, chips * share)], near.at[index], ss.at[0], sr.at[index],
             device_id=sibling, device_id_type=MESH)
 
     def back(index, j):
         at = index * (chips - 1) + j - 1
         return pltpu.make_async_remote_copy(
-            pair.at[index, chip(j)], far.at[index, j - 1], bs.at[at], br.at[at],
+            pair.at[index, chip(j)], far.at[index, j - 1], bs.at[j - 1], br.at[at],
             device_id=(g, f, 2 * chip(j) + c), device_id_type=MESH)
 
-    def stage(which, period):
+    def stage(which, period, low=0, high=5):
         def one(slot, carry):
             exists, m, index = slot_of(period, slot)
 
@@ -273,7 +280,7 @@
                     out[index] = value.astype(jnp.bfloat16)
             return carry
 
-        lax.fori_loop(0, 5, one, 0)
+        lax.fori_loop(low, high, one, 0)
 
     def forward(s):
         m, j = lax.div(s, span), lax.rem(s, span)
@@ -300,16 +307,10 @@
                 @pl.when(has[way])
                 def _():
                     along(way, m, k, q).start()
-                across(m, origin(way, k), g, q, x_at(way, m, k, q)).start()
-
-    def absorb(i):
-        @pl.when(i < total)
-        def _():
-            _, source, xq = x_of(i)
-            across(0, source, other, xq, i).wait_recv()
-
-        period, p = lax.div(i, per_block), lax.rem(i, per_block)
-
+                across(
+                    m, origin(way, k), g, q, (way * 2 + m) * last + k - 1, x_at(way, m, k, q)).start()
+
+    def run(period, low, high, first, end):
         def one(slot, carry):
             exists, m, index = slot_of(period, slot)
 
@@ -318,68 +319,92 @@
                 def body(r, carry):
                     multiply(m, index, slot, r)
                     return carry
-                lax.fori_loop(p * each, jnp.minimum((p + 1) * each, pieces), body, 0)
+                lax.fori_loop(first, end, body, 0)
             return carry
 
-        lax.fori_loop(0, 5, one, 0)
+        lax.fori_loop(low, high, one, 0)
+
+    def absorb(i, low, high, wait):
+        if wait:
+            _, source, xq = x_of(i)
+            across(0, source, other, xq, 0, i).wait_recv()
+        period, p = lax.div(i, per_block), lax.rem(i, per_block)
+        run(period, low, high, jnp.minimum(p * each, pieces), jnp.minimum((p + 1) * each, pieces))
 
         @pl.when(p == per_block - 1)
         def _():
-            stage(0, period)
-            stage(2, period - 1)
-            stage(1, period)
-            stage(3, period - 1)
-            stage(4, period - 2)
-
-        @pl.when(i == span + per_block - 1)
-        def _():
-            for r in range(pieces):
-                hidden[r] = jnp.square(jnp.maximum(acc[r], 0.0)).astype(jnp.bfloat16)
+            stage(0, period, low, high)
+            if wait:
+                stage(2, period - 1)
+            stage(1, period, low, high)
+            if wait:
+                stage(3, period - 1)
+                stage(4, period - 2)
+
+        if wait:
+            @pl.when(i == span + per_block - 1)
+            def _():
+                for r in range(pieces):
+                    hidden[r] = jnp.square(jnp.maximum(acc[r], 0.0)).astype(jnp.bfloat16)
 
     def step(s, carry):
-        @pl.when(s < total)
-        def _():
-            forward(s)
+        forward(s)
 
         @pl.when(s >= LAG)
         def _():
-            absorb(s - LAG)
+            absorb(s - LAG, 0, 5, True)
         return carry
 
-    lax.fori_loop(0, total + LAG + per_block, step, 0)
+    lax.fori_loop(0, total, step, 0)
     final = total // per_block
+
+    def drain(low, high, wait):
+        def one(i, carry):
+            absorb(i, low, high, wait)
+            return carry
+
+        lax.fori_loop(total - LAG, total, one, 0)
+        run(final, low, high, 0, pieces)
+        stage(0, final, low, high)
+        stage(1, final, low, high)
+
+    drain(0, 2, False)
+    drain(2, 5, True)
+    stage(2, final - 1)
+    stage(3, final - 1)
     stage(2, final)
     stage(3, final)
+    stage(4, final - 2)
     stage(4, final - 1)
     stage(4, final)
 
-    def finish(s, carry):
-        m, j = lax.div(s, span), lax.rem(s, span)
-        k, q = lax.div(j, count), lax.rem(j, count)
+    def finish(r, carry):
+        m, k = lax.div(r, last), lax.rem(r, last)
         for way in range(2):
             @pl.when(has[way] & ((k == 0) | reach(way, k)))
             def _(way=way):
-                along(way, m, k, q).wait_send()
-        _, source, xq = x_of(s)
-        across(m, source, g, xq, s).wait_send()
+                all_rows(m, origin(way, k), way, k, False).wait_send()
+
+            @pl.when(reach(way, k + 1))
+            def _(way=way):
+                all_rows(m, origin(way, k + 1), way, k, True).wait_send()
         return carry
 
-    lax.fori_loop(0, total, finish, 0)
-
-    def finish_sum(index, carry):
-        over(index).wait_send()
-        for j in range(1, chips):
-            back(index, j).wait_send()
-        return carry
-
-    lax.fori_loop(0, n * every, finish_sum, 0)
+    lax.fori_loop(0, 2 * last, finish, 0)
+    pltpu.make_async_remote_copy(
+        part.at[:, pl.ds(theirs, chips * share)], near, ss.at[0], sr.at[0],
+        device_id=sibling, device_id_type=MESH).wait_send()
+    for j in range(1, chips):
+        pltpu.make_async_remote_copy(
+            pair.at[:, chip(j)], far.at[:, j - 1], bs.at[j - 1], br.at[0],
+            device_id=(g, f, 2 * chip(j) + c), device_id_type=MESH).wait_send()
 
 
 def gather(n, tp, tokens, gain, up, down):
     local, width = up.shape
     count_rows = tokens.shape[0]
     half = local // 2
-    block = divisor(half, 128, 16)
+    block = divisor(half, 256, 16)
     rows = chunk_rows(block, width)
     count = half // rows
     depth = n * local
@@ -414,13 +439,13 @@
             pltpu.VMEM((total, chips - 1, share, block), jnp.bfloat16),
             dma((min(SLOTS, 4 * count),)),
             dma((1,)),
+            dma((4 * (n - 1),)),
             dma((2 * moves,)),
-            dma((2 * moves,)),
+            dma((4 * (n - 1),)),
             dma((moves,)),
-            dma((moves,)),
+            dma((1,)),
             dma((total,)),
-            dma((total,)),
-            dma((total * (chips - 1),)),
+            dma((chips - 1,)),
             dma((total * (chips - 1),)),
         ],
         compiler_params=pltpu.CompilerParams(

time: 471 us -> 454 us (0.964)
  Pallas kernels: 470 us -> 453 us
    pallas_call x1, Pallas kernels: 453 us -> 436 us  [gather(): pl.pallas_call(functools.partial(gather_kernel, (n, tp, local, block, row...]
where the time goes in v3:
time: 454 us
  Pallas kernels  453 us (100%)
    pallas_call x1, Pallas kernels, gather(): pl.pallas_call(functools.partial(gather_kernel, (n, tp, local, block, row...  436 us
    pallas_call x1, Pallas kernels, per_device(): pl.pallas_call(functools.partial(write_kernel, parts), out_shape=[weight,...  17.2 us

profile of v3, /device:TPU:0, one launch (start us, length us, event | category | flops | bytes accessed | tf_op | source)
XLA Modules:
  0.0 454.1 jit_solution(11232440561384704152)
XLA Ops:
  0.6 436.3 %gather_both.1 = (bf16[2,3584,3584]{2,1,0:T(8,128)(2,1)S(1)}, bf16[16,32,224]{2,1,0:T(8,128)(2,1)S(1)}) custom-call(bf16[128,3584]{1,0:T(8,128)(2,1)} %tokens.1, f32[7,128]{1,0:T(8,128)} %bitcast.1, f32[896,3584]{1,0:T(8,128)} %up.1, f32[896,3584]{1,0:T(8,128)} %down.1), custom_call_target="tpu_custom_call" | custom-call | bytes 57802752 | tf_op jit(solution)/shard_map/gather_both/pallas_call | solution.py:419
  436.9 17.2 %write_out.1 = (bf16[3584,3584]{1,0:T(8,128)(2,1)}, bf16[3584,3584]{1,0:T(8,128)(2,1)}, bf16[32,3584]{1,0:T(8,128)(2,1)}) custom-call(bf16[2,3584,3584]{2,1,0:T(8,128)(2,1)S(1)} %get-tuple-element.5.both, bf16[16,32,224]{2,1,0:T(8,128)(2,1)S(1)} %get-tuple-element.6.mixed), custom_call_target="tpu_custom_call" | custom-call | tf_op jit(solution)/shard_map/write_out/pallas_call | solution.py:483

commit v4 on v3

--- a/solution.py
+++ b/solution.py
@@ -27,7 +27,7 @@
 
 
 def gather_kernel(sizes, tokens, gain, up, down, both, out, wide, column, held, normed, acc, hidden, product,
-                  part, near, pair, kept, far, load, token_s, zs, zr, xs, xr, ss, sr, bs, br):
+                  ending, part, far, load, token_s, zs, zr, xs, xr, ss, sr):
     n, tp, local, block, rows, piece = sizes
     half = local // 2
     count = half // rows
@@ -39,10 +39,9 @@
     slots = wide.shape[0]
     g, f, t = lax.axis_index("grp"), lax.axis_index("fs"), lax.axis_index("tp")
     other = 1 - g
-    chips = tp // 2
-    y, c = t // 2, lax.rem(t, 2)
     every = 2 * blocks
-    share = kept.shape[1]
+    share = part.shape[2]
+    final = total // per_block
     pieces = acc.shape[0]
     each = -(-pieces // per_block)
     double = jnp.minimum(f, last - f)
@@ -150,14 +149,12 @@
         def _(way=way):
             pl.semaphore_signal(barrier, inc=1, device_id=hop(way), device_id_type=MESH)
     pl.semaphore_signal(barrier, inc=1, device_id=(other, f, t), device_id_type=MESH)
-    sibling = (g, f, 2 * y + 1 - c)
-    pl.semaphore_signal(barrier, inc=1, device_id=sibling, device_id_type=MESH)
-
-    def chip(j):
-        return lax.rem(y + j, chips)
-
-    for j in range(1, chips):
-        pl.semaphore_signal(barrier, inc=1, device_id=(g, f, 2 * chip(j) + c), device_id_type=MESH)
+
+    def mate(j):
+        return lax.rem(t + j, tp)
+
+    for j in range(1, tp):
+        pl.semaphore_signal(barrier, inc=1, device_id=(g, f, mate(j)), device_id_type=MESH)
     step_rows = divisor(local, 128, 8)
     eye = lax.broadcasted_iota(jnp.int32, (step_rows, step_rows), 0) == lax.broadcasted_iota(
         jnp.int32, (step_rows, step_rows), 1)
@@ -165,7 +162,7 @@
         line = gain[i:i + 1, :]
         column[i * step_rows:(i + 1) * step_rows, :] = jnp.sum(
             jnp.where(eye, line, 0.0), axis=1, keepdims=True)
-    pl.semaphore_wait(barrier, 1 + chips + jnp.minimum(f, 1) + jnp.minimum(last - f, 1))
+    pl.semaphore_wait(barrier, tp + jnp.minimum(f, 1) + jnp.minimum(last - f, 1))
 
     def first_step(q, carry):
         convert(0, g, q, q)
@@ -181,8 +178,6 @@
     square_mean = jnp.mean(values * values, axis=1, keepdims=True)
     send_own(0, count - 1)
     scaled = (values * lax.rsqrt(square_mean + 1e-06)).astype(jnp.bfloat16)
-    scaled = jnp.concatenate(
-        [scaled[i * share:(i + 1) * share] for i in list(range(0, tp, 2)) + list(range(1, tp, 2))])
     for i in range(normed.shape[0]):
         normed[i] = scaled[:, i * block:(i + 1) * block]
     acc[...] = jnp.zeros_like(acc)
@@ -235,19 +230,11 @@
             def _():
                 product[slot] += value
 
-    mine = pl.multiple_of(c * (chips * share), 4)
-    theirs = pl.multiple_of((1 - c) * (chips * share), 4)
-
-    def over(index):
+    def share_out(index, j):
+        at = index * (tp - 1) + j - 1
         return pltpu.make_async_remote_copy(
-            part.at[index, pl.ds(theirs, chips * share)], near.at[index], ss.at[0], sr.at[index],
-            device_id=sibling, device_id_type=MESH)
-
-    def back(index, j):
-        at = index * (chips - 1) + j - 1
-        return pltpu.make_async_remote_copy(
-            pair.at[index, chip(j)], far.at[index, j - 1], bs.at[j - 1], br.at[at],
-            device_id=(g, f, 2 * chip(j) + c), device_id_type=MESH)
+            part.at[index, mate(j)], far.at[index, j - 1], ss.at[j - 1], sr.at[at],
+            device_id=(g, f, mate(j)), device_id_type=MESH)
 
     def stage(which, period, low=0, high=5):
         def one(slot, carry):
@@ -256,26 +243,15 @@
             @pl.when(exists & (m == 1))
             def _():
                 if which == 0:
-                    part[index] = product[slot].astype(jnp.bfloat16)
+                    for j in range(tp):
+                        part[index, j] = product[slot, j * share:(j + 1) * share].astype(jnp.bfloat16)
                 elif which == 1:
-                    over(index).start()
-                elif which == 2:
-                    over(index).wait_recv()
-                    value = part[index, pl.ds(mine, chips * share)].astype(jnp.float32) + near[index].astype(jnp.float32)
-                    for j in range(chips):
-                        rows_j = value[j * share:(j + 1) * share]
-                        pair[index, j] = rows_j.astype(jnp.bfloat16)
-
-                        @pl.when(y == j)
-                        def _(rows_j=rows_j):
-                            kept[index] = rows_j
-                elif which == 3:
-                    for j in range(1, chips):
-                        back(index, j).start()
+                    for j in range(1, tp):
+                        share_out(index, j).start()
                 else:
-                    value = kept[index]
-                    for j in range(1, chips):
-                        back(index, j).wait_recv()
+                    value = part[index, t].astype(jnp.float32)
+                    for j in range(1, tp):
+                        share_out(index, j).wait_recv()
                         value = value + far[index, j - 1].astype(jnp.float32)
                     out[index] = value.astype(jnp.bfloat16)
             return carry
@@ -328,18 +304,25 @@
         if wait:
             _, source, xq = x_of(i)
             across(0, source, other, xq, 0, i).wait_recv()
+
+            @pl.when((i >= total - per_block) & (n % 2 == 0))
+            def _():
+                first = pl.multiple_of(source * local + other * half + xq * rows, 16)
+                value = jnp.zeros(ending.shape[1:], jnp.float32)
+                for p in range(pieces):
+                    value = value + lax.dot_general(
+                        hidden[p], both[1, pl.ds(first, rows), p * piece:(p + 1) * piece],
+                        (((1,), (1,)), ((), ())), preferred_element_type=jnp.float32)
+                ending[lax.rem(i, per_block)] = value
         period, p = lax.div(i, per_block), lax.rem(i, per_block)
         run(period, low, high, jnp.minimum(p * each, pieces), jnp.minimum((p + 1) * each, pieces))
 
         @pl.when(p == per_block - 1)
         def _():
             stage(0, period, low, high)
+            stage(1, period, low, high)
             if wait:
                 stage(2, period - 1)
-            stage(1, period, low, high)
-            if wait:
-                stage(3, period - 1)
-                stage(4, period - 2)
 
         if wait:
             @pl.when(i == span + per_block - 1)
@@ -356,27 +339,27 @@
         return carry
 
     lax.fori_loop(0, total, step, 0)
-    final = total // per_block
-
     def drain(low, high, wait):
         def one(i, carry):
             absorb(i, low, high, wait)
             return carry
 
         lax.fori_loop(total - LAG, total, one, 0)
-        run(final, low, high, 0, pieces)
-        stage(0, final, low, high)
-        stage(1, final, low, high)
 
     drain(0, 2, False)
+    run(final, 0, 2, 0, pieces)
+    stage(0, final, 0, 2)
+    stage(1, final, 0, 2)
     drain(2, 5, True)
+    if n % 2 == 0:
+        for p in range(per_block):
+            product[2, :, p * rows:(p + 1) * rows] = ending[p]
+    else:
+        run(final, 2, 4, 0, pieces)
+    stage(0, final, 2, 4)
+    stage(1, final, 2, 4)
     stage(2, final - 1)
-    stage(3, final - 1)
-    stage(2, final)
-    stage(3, final)
-    stage(4, final - 2)
-    stage(4, final - 1)
-    stage(4, final)
+    stage(2, final, 0, 4)
 
     def finish(r, carry):
         m, k = lax.div(r, last), lax.rem(r, last)
@@ -391,13 +374,10 @@
         return carry
 
     lax.fori_loop(0, 2 * last, finish, 0)
-    pltpu.make_async_remote_copy(
-        part.at[:, pl.ds(theirs, chips * share)], near, ss.at[0], sr.at[0],
-        device_id=sibling, device_id_type=MESH).wait_send()
-    for j in range(1, chips):
+    for j in range(1, tp):
         pltpu.make_async_remote_copy(
-            pair.at[:, chip(j)], far.at[:, j - 1], bs.at[j - 1], br.at[0],
-            device_id=(g, f, 2 * chip(j) + c), device_id_type=MESH).wait_send()
+            part.at[:, mate(j)], far.at[:, j - 1], ss.at[j - 1], sr.at[0],
+            device_id=(g, f, mate(j)), device_id_type=MESH).wait_send()
 
 
 def gather(n, tp, tokens, gain, up, down):
@@ -410,7 +390,7 @@
     depth = n * local
     piece = next(size for size in (512, 256, 128, width) if width % size == 0)
     moves = 2 * (n - 1) * count
-    share, chips, total = count_rows // tp, tp // 2, depth // block
+    share, total = count_rows // tp, depth // block
     dma = pltpu.SemaphoreType.DMA
     step_rows = divisor(local, 128, 8)
     sent = 3 * (n - 1) * local * width * 2
@@ -432,21 +412,17 @@
             pltpu.VMEM((width // piece, count_rows, piece), jnp.float32),
             pltpu.VMEM((width // piece, count_rows, piece), jnp.bfloat16),
             pltpu.VMEM((5, count_rows, block), jnp.float32),
-            pltpu.VMEM((total, count_rows, block), jnp.bfloat16),
-            pltpu.VMEM((total, count_rows // 2, block), jnp.bfloat16),
-            pltpu.VMEM((total, chips, share, block), jnp.bfloat16),
-            pltpu.VMEM((total, share, block), jnp.float32),
-            pltpu.VMEM((total, chips - 1, share, block), jnp.bfloat16),
+            pltpu.VMEM((block // rows, count_rows, rows), jnp.float32),
+            pltpu.VMEM((total, tp, share, block), jnp.bfloat16),
+            pltpu.VMEM((total, tp - 1, share, block), jnp.bfloat16),
             dma((min(SLOTS, 4 * count),)),
             dma((1,)),
             dma((4 * (n - 1),)),
             dma((2 * moves,)),
             dma((4 * (n - 1),)),
             dma((moves,)),
-            dma((1,)),
-            dma((total,)),
-            dma((chips - 1,)),
-            dma((total * (chips - 1),)),
+            dma((tp - 1,)),
+            dma((total * (tp - 1),)),
         ],
         compiler_params=pltpu.CompilerParams(
             collective_id=0, has_side_effects=True, vmem_limit_bytes=27 * 512 * 1024),

time: 454 us -> 452 us (level)
  no operation moved by 1% of the time
where the time goes in v4:
time: 452 us
  Pallas kernels  451 us (100%)
    pallas_call x1, Pallas kernels, gather(): pl.pallas_call(functools.partial(gather_kernel, (n, tp, local, block, row...  434 us
    pallas_call x1, Pallas kernels, per_device(): pl.pallas_call(functools.partial(write_kernel, parts), out_shape=[weight,...  17.2 us

profile of v4, /device:TPU:0, one launch (start us, length us, event | category | flops | bytes accessed | tf_op | source)
XLA Modules:
  0.0 451.5 jit_solution(6662124557140539107)
XLA Ops:
  0.6 433.7 %gather_both.1 = (bf16[2,3584,3584]{2,1,0:T(8,128)(2,1)S(1)}, bf16[16,32,224]{2,1,0:T(8,128)(2,1)S(1)}) custom-call(bf16[128,3584]{1,0:T(8,128)(2,1)} %tokens.1, f32[7,128]{1,0:T(8,128)} %bitcast.1, f32[896,3584]{1,0:T(8,128)} %up.1, f32[896,3584]{1,0:T(8,128)} %down.1), custom_call_target="tpu_custom_call" | custom-call | bytes 57802752 | tf_op jit(solution)/shard_map/gather_both/pallas_call | solution.py:399
  434.3 17.2 %write_out.1 = (bf16[3584,3584]{1,0:T(8,128)(2,1)}, bf16[3584,3584]{1,0:T(8,128)(2,1)}, bf16[32,3584]{1,0:T(8,128)(2,1)}) custom-call(bf16[2,3584,3584]{2,1,0:T(8,128)(2,1)S(1)} %get-tuple-element.5.both, bf16[16,32,224]{2,1,0:T(8,128)(2,1)S(1)} %get-tuple-element.6.mixed), custom_call_target="tpu_custom_call" | custom-call | tf_op jit(solution)/shard_map/write_out/pallas_call | solution.py:459

commit v5 on v4

--- a/solution.py
+++ b/solution.py
@@ -27,7 +27,7 @@
 
 
 def gather_kernel(sizes, tokens, gain, up, down, both, out, wide, column, held, normed, acc, hidden, product,
-                  ending, part, far, load, token_s, zs, zr, xs, xr, ss, sr):
+                  ending, part, far, load, token_s, zs, zr, xs, xr, es, er, ss, sr):
     n, tp, local, block, rows, piece = sizes
     half = local // 2
     count = half // rows
@@ -42,6 +42,7 @@
     every = 2 * blocks
     share = part.shape[2]
     final = total // per_block
+    extra = rows // 32 * 16
     pieces = acc.shape[0]
     each = -(-pieces // per_block)
     double = jnp.minimum(f, last - f)
@@ -100,8 +101,19 @@
             place, place, zs.at[(way * 2 + m) * last + k], zr.at[z_at(way, m, k, q)],
             device_id=hop(way), device_id_type=MESH)
 
-    def all_rows(m, source, way, k, across_x):
-        place = both.at[m, pl.ds(pl.multiple_of(source * local + g * half, 16), half)]
+    ends = (0, last)
+
+    def shortened(m, source, q):
+        return (m == 1) & (q == count - 1) & ((source == 0) | (source == last)) & (extra > 0)
+
+    def extra_rows(way, source):
+        first = pl.multiple_of(source * local + other * half + half - extra, 16)
+        place = both.at[1, pl.ds(first, extra)]
+        return pltpu.make_async_remote_copy(
+            place, place, es.at[way], er.at[way], device_id=hop(way), device_id_type=MESH)
+
+    def all_rows(m, source, way, k, across_x, size):
+        place = both.at[m, pl.ds(pl.multiple_of(source * local + g * half, 16), size)]
         at = (way * 2 + m) * last + k
         return pltpu.make_async_remote_copy(
             place, place, (xs if across_x else zs).at[at], zr.at[0],
@@ -128,8 +140,9 @@
         source = f + (2 * up_side - 1) * k
         return m, source, q
 
-    def across(m, source, which, q, sent, i):
-        place = where(m, source, which, q)
+    def across(m, source, which, q, sent, i, size=rows):
+        first = pl.multiple_of(source * local + which * half + q * rows, 16)
+        place = both.at[m, pl.ds(first, size)]
         return pltpu.make_async_remote_copy(
             place, place, xs.at[sent], xr.at[i], device_id=(other, f, t), device_id_type=MESH)
 
@@ -275,6 +288,12 @@
         def _():
             send_own(1, s - 1 - (span - count))
 
+        if extra:
+            for way in range(2):
+                @pl.when((s == span) & (f == ends[way]))
+                def _(way=way):
+                    extra_rows(way, f).start()
+
         for way in range(2):
             @pl.when(reach(way, k))
             def _(way=way):
@@ -283,8 +302,23 @@
                 @pl.when(has[way])
                 def _():
                     along(way, m, k, q).start()
-                across(
-                    m, origin(way, k), g, q, (way * 2 + m) * last + k - 1, x_at(way, m, k, q)).start()
+                short = shortened(m, origin(way, k), q)
+                for size, chosen in ((rows, ~short), (rows - extra, short)):
+                    @pl.when(chosen)
+                    def _(size=size):
+                        across(
+                            m, origin(way, k), g, q, (way * 2 + m) * last + k - 1,
+                            x_at(way, m, k, q), size).start()
+
+        if extra:
+            for way in range(2):
+                @pl.when((m == 1) & (q == count - 1) & reach(way, k) & (origin(way, k) == ends[way]))
+                def _(way=way):
+                    extra_rows(way, ends[way]).wait_recv()
+
+                    @pl.when(has[way])
+                    def _():
+                        extra_rows(way, ends[way]).start()
 
     def run(period, low, high, first, end):
         def one(slot, carry):
@@ -300,20 +334,40 @@
 
         lax.fori_loop(low, high, one, 0)
 
+    def take(i):
+        m = lax.div(i, span)
+        _, source, xq = x_of(i)
+        short = shortened(m, source, xq)
+        for size, chosen in ((rows, ~short), (rows - extra, short)):
+            @pl.when(chosen)
+            def _(size=size):
+                across(0, source, other, xq, 0, i, size).wait_recv()
+        return source, xq
+
+    def chunk_product(source, xq):
+        first = pl.multiple_of(source * local + other * half + xq * rows, 16)
+        value = jnp.zeros(ending.shape[1:], jnp.float32)
+        for p in range(pieces):
+            value = value + lax.dot_general(
+                hidden[p], both[1, pl.ds(first, rows), p * piece:(p + 1) * piece],
+                (((1,), (1,)), ((), ())), preferred_element_type=jnp.float32)
+        return value
+
+    single = n % 2 == 0
+
+    def take_and_multiply(i):
+        source, xq = take(i)
+        if single:
+            @pl.when(i >= total - per_block)
+            def _():
+                ending[lax.rem(i, per_block)] = chunk_product(source, xq)
+
     def absorb(i, low, high, wait):
         if wait:
-            _, source, xq = x_of(i)
-            across(0, source, other, xq, 0, i).wait_recv()
-
-            @pl.when((i >= total - per_block) & (n % 2 == 0))
-            def _():
-                first = pl.multiple_of(source * local + other * half + xq * rows, 16)
-                value = jnp.zeros(ending.shape[1:], jnp.float32)
-                for p in range(pieces):
-                    value = value + lax.dot_general(
-                        hidden[p], both[1, pl.ds(first, rows), p * piece:(p + 1) * piece],
-                        (((1,), (1,)), ((), ())), preferred_element_type=jnp.float32)
-                ending[lax.rem(i, per_block)] = value
+            take_and_multiply(i)
+        rest(i, low, high, wait)
+
+    def rest(i, low, high, wait):
         period, p = lax.div(i, per_block), lax.rem(i, per_block)
         run(period, low, high, jnp.minimum(p * each, pieces), jnp.minimum((p + 1) * each, pieces))
 
@@ -339,41 +393,70 @@
         return carry
 
     lax.fori_loop(0, total, step, 0)
-    def drain(low, high, wait):
+    def drain(low, high, wait, end):
         def one(i, carry):
             absorb(i, low, high, wait)
             return carry
 
-        lax.fori_loop(total - LAG, total, one, 0)
-
-    drain(0, 2, False)
-    run(final, 0, 2, 0, pieces)
-    stage(0, final, 0, 2)
-    stage(1, final, 0, 2)
-    drain(2, 5, True)
-    if n % 2 == 0:
-        for p in range(per_block):
-            product[2, :, p * rows:(p + 1) * rows] = ending[p]
-    else:
-        run(final, 2, 4, 0, pieces)
-    stage(0, final, 2, 4)
-    stage(1, final, 2, 4)
-    stage(2, final - 1)
-    stage(2, final, 0, 4)
+        lax.fori_loop(total - LAG, end, one, 0)
 
     def finish(r, carry):
         m, k = lax.div(r, last), lax.rem(r, last)
         for way in range(2):
             @pl.when(has[way] & ((k == 0) | reach(way, k)))
             def _(way=way):
-                all_rows(m, origin(way, k), way, k, False).wait_send()
-
-            @pl.when(reach(way, k + 1))
-            def _(way=way):
-                all_rows(m, origin(way, k + 1), way, k, True).wait_send()
+                all_rows(m, origin(way, k), way, k, False, half).wait_send()
+
+            short = shortened(m, origin(way, k + 1), count - 1)
+            for size, chosen in ((half, ~short), (half - extra, short)):
+                @pl.when(reach(way, k + 1) & chosen)
+                def _(way=way, size=size):
+                    all_rows(m, origin(way, k + 1), way, k, True, size).wait_send()
         return carry
 
-    lax.fori_loop(0, 2 * last, finish, 0)
+    def finish_all():
+        lax.fori_loop(0, 2 * last, finish, 0)
+        if extra:
+            for way in range(2):
+                @pl.when(has[way])
+                def _(way=way):
+                    extra_rows(way, ends[way]).wait_send()
+
+    drain(0, 2, False, total)
+    run(final, 0, 2, 0, pieces)
+    stage(0, final, 0, 2)
+    stage(1, final, 0, 2)
+    if single:
+        drain(2, 5, True, total - 1)
+        rest(total - 1, 2, 5, True)
+        stage(2, final - 1)
+        _, source, _ = x_of(total - 1)
+        index = source * every + other * blocks + blocks - 1
+        for p in range(per_block - 1):
+            value = ending[p].astype(jnp.bfloat16)
+            for j in range(tp):
+                part[index, j, :, p * rows:(p + 1) * rows] = value[j * share:(j + 1) * share]
+        take(total - 1)
+        value = chunk_product(source, count - 1).astype(jnp.bfloat16)
+        for j in range(tp):
+            part[index, j, :, (per_block - 1) * rows:] = value[j * share:(j + 1) * share]
+        for j in range(1, tp):
+            share_out(index, j).start()
+        finish_all()
+        stage(2, final, 0, 2)
+        value = part[index, t].astype(jnp.float32)
+        for j in range(1, tp):
+            share_out(index, j).wait_recv()
+            value = value + far[index, j - 1].astype(jnp.float32)
+        out[index] = value.astype(jnp.bfloat16)
+    else:
+        drain(2, 5, True, total)
+        run(final, 2, 4, 0, pieces)
+        stage(0, final, 2, 4)
+        stage(1, final, 2, 4)
+        finish_all()
+        stage(2, final - 1)
+        stage(2, final, 0, 4)
     for j in range(1, tp):
         pltpu.make_async_remote_copy(
             part.at[:, mate(j)], far.at[:, j - 1], ss.at[j - 1], sr.at[0],
@@ -421,6 +504,8 @@
             dma((2 * moves,)),
             dma((4 * (n - 1),)),
             dma((moves,)),
+            dma((2,)),
+            dma((2,)),
             dma((tp - 1,)),
             dma((total * (tp - 1),)),
         ],

time: 452 us -> 455 us (level)
  no operation moved by 1% of the time
where the time goes in v5:
time: 455 us
  Pallas kernels  454 us (100%)
    pallas_call x1, Pallas kernels, gather(): pl.pallas_call(functools.partial(gather_kernel, (n, tp, local, block, row...  437 us
    pallas_call x1, Pallas kernels, per_device(): pl.pallas_call(functools.partial(write_kernel, parts), out_shape=[weight,...  17.2 us

profile of v5, /device:TPU:0, one launch (start us, length us, event | category | flops | bytes accessed | tf_op | source)
XLA Modules:
  0.0 454.7 jit_solution(362726259340288369)
XLA Ops:
  0.6 436.8 %gather_both.1 = (bf16[2,3584,3584]{2,1,0:T(8,128)(2,1)S(1)}, bf16[16,32,224]{2,1,0:T(8,128)(2,1)S(1)}) custom-call(bf16[128,3584]{1,0:T(8,128)(2,1)} %tokens.1, f32[7,128]{1,0:T(8,128)} %bitcast.1, f32[896,3584]{1,0:T(8,128)} %up.1, f32[896,3584]{1,0:T(8,128)} %down.1), custom_call_target="tpu_custom_call" | custom-call | bytes 57802752 | tf_op jit(solution)/shard_map/gather_both/pallas_call | solution.py:482
  437.5 17.2 %write_out.1 = (bf16[3584,3584]{1,0:T(8,128)(2,1)}, bf16[3584,3584]{1,0:T(8,128)(2,1)}, bf16[32,3584]{1,0:T(8,128)(2,1)}) custom-call(bf16[2,3584,3584]{2,1,0:T(8,128)(2,1)S(1)} %get-tuple-element.5.both, bf16[16,32,224]{2,1,0:T(8,128)(2,1)S(1)} %get-tuple-element.6.mixed), custom_call_target="tpu_custom_call" | custom-call | tf_op jit(solution)/shard_map/write_out/pallas_call | solution.py:544

commit v6 on v5

--- a/solution.py
+++ b/solution.py
@@ -44,7 +44,9 @@
     final = total // per_block
     extra = rows // 32 * 16
     pieces = acc.shape[0]
-    each = -(-pieces // per_block)
+    trigger = per_block - 1 - LAG if per_block > 2 * LAG else per_block - 1
+    each = -(-pieces // (trigger + 1))
+    single = n % 2 == 0
     double = jnp.minimum(f, last - f)
 
     def start_load(m, which, q, index):
@@ -271,6 +273,15 @@
 
         lax.fori_loop(low, high, one, 0)
 
+    def chunk_product(source, which, q):
+        first = pl.multiple_of(source * local + which * half + q * rows, 16)
+        value = jnp.zeros(ending.shape[2:], jnp.float32)
+        for p in range(pieces):
+            value = value + lax.dot_general(
+                hidden[p], both[1, pl.ds(first, rows), p * piece:(p + 1) * piece],
+                (((1,), (1,)), ((), ())), preferred_element_type=jnp.float32)
+        return value
+
     def forward(s):
         m, j = lax.div(s, span), lax.rem(s, span)
         k, q = 1 + lax.div(j, count), lax.rem(j, count)
@@ -312,13 +323,15 @@
 
         if extra:
             for way in range(2):
-                @pl.when((m == 1) & (q == count - 1) & reach(way, k) & (origin(way, k) == ends[way]))
+                @pl.when((m == 1) & (q == count - 1) & reach(way, k) & (origin(way, k) == ends[way]) & has[way])
                 def _(way=way):
                     extra_rows(way, ends[way]).wait_recv()
-
-                    @pl.when(has[way])
-                    def _():
-                        extra_rows(way, ends[way]).start()
+                    extra_rows(way, ends[way]).start()
+
+        if single:
+            @pl.when((s >= total - per_block) & (reach(0, k) | reach(1, k)))
+            def _():
+                ending[1, lax.rem(q, per_block)] = chunk_product(last - f, g, q)
 
     def run(period, low, high, first, end):
         def one(slot, carry):
@@ -344,23 +357,12 @@
                 across(0, source, other, xq, 0, i, size).wait_recv()
         return source, xq
 
-    def chunk_product(source, xq):
-        first = pl.multiple_of(source * local + other * half + xq * rows, 16)
-        value = jnp.zeros(ending.shape[1:], jnp.float32)
-        for p in range(pieces):
-            value = value + lax.dot_general(
-                hidden[p], both[1, pl.ds(first, rows), p * piece:(p + 1) * piece],
-                (((1,), (1,)), ((), ())), preferred_element_type=jnp.float32)
-        return value
-
-    single = n % 2 == 0
-
     def take_and_multiply(i):
         source, xq = take(i)
         if single:
             @pl.when(i >= total - per_block)
             def _():
-                ending[lax.rem(i, per_block)] = chunk_product(source, xq)
+                ending[0, lax.rem(i, per_block)] = chunk_product(source, other, xq)
 
     def absorb(i, low, high, wait):
         if wait:
@@ -369,9 +371,12 @@
 
     def rest(i, low, high, wait):
         period, p = lax.div(i, per_block), lax.rem(i, per_block)
-        run(period, low, high, jnp.minimum(p * each, pieces), jnp.minimum((p + 1) * each, pieces))
-
-        @pl.when(p == per_block - 1)
+
+        @pl.when(p <= trigger)
+        def _():
+            run(period, low, high, jnp.minimum(p * each, pieces), jnp.minimum((p + 1) * each, pieces))
+
+        @pl.when(p == trigger)
         def _():
             stage(0, period, low, high)
             stage(1, period, low, high)
@@ -379,7 +384,7 @@
                 stage(2, period - 1)
 
         if wait:
-            @pl.when(i == span + per_block - 1)
+            @pl.when(i == span + trigger)
             def _():
                 for r in range(pieces):
                     hidden[r] = jnp.square(jnp.maximum(acc[r], 0.0)).astype(jnp.bfloat16)
@@ -422,38 +427,64 @@
                 def _(way=way):
                     extra_rows(way, ends[way]).wait_send()
 
+    def take_extra():
+        if extra:
+            for way in range(2):
+                @pl.when(f == ends[1 - way])
+                def _(way=way):
+                    extra_rows(way, ends[way]).wait_recv()
+
+    def fill(which, index, low, high):
+        for p in range(low, high):
+            value = ending[which, p].astype(jnp.bfloat16)
+            for j in range(tp):
+                part[index, j, :, p * rows:(p + 1) * rows] = value[j * share:(j + 1) * share]
+
+    def share_all(index):
+        for j in range(1, tp):
+            share_out(index, j).start()
+
+    def collect(index):
+        value = part[index, t].astype(jnp.float32)
+        for j in range(1, tp):
+            share_out(index, j).wait_recv()
+            value = value + far[index, j - 1].astype(jnp.float32)
+        out[index] = value.astype(jnp.bfloat16)
+
     drain(0, 2, False, total)
-    run(final, 0, 2, 0, pieces)
-    stage(0, final, 0, 2)
-    stage(1, final, 0, 2)
     if single:
+        far_end = (f == 0) | (f == last)
+        z_index = (last - f) * every + g * blocks + blocks - 1
+
+        @pl.when(far_end)
+        def _():
+            fill(1, z_index, 0, per_block)
+            share_all(z_index)
+
         drain(2, 5, True, total - 1)
         rest(total - 1, 2, 5, True)
         stage(2, final - 1)
         _, source, _ = x_of(total - 1)
         index = source * every + other * blocks + blocks - 1
-        for p in range(per_block - 1):
-            value = ending[p].astype(jnp.bfloat16)
-            for j in range(tp):
-                part[index, j, :, p * rows:(p + 1) * rows] = value[j * share:(j + 1) * share]
+        fill(0, index, 0, per_block - 1)
+        take_extra()
         take(total - 1)
-        value = chunk_product(source, count - 1).astype(jnp.bfloat16)
-        for j in range(tp):
-            part[index, j, :, (per_block - 1) * rows:] = value[j * share:(j + 1) * share]
-        for j in range(1, tp):
-            share_out(index, j).start()
+        ending[0, per_block - 1] = chunk_product(source, other, count - 1)
+        fill(0, index, per_block - 1, per_block)
+        share_all(index)
         finish_all()
-        stage(2, final, 0, 2)
-        value = part[index, t].astype(jnp.float32)
-        for j in range(1, tp):
-            share_out(index, j).wait_recv()
-            value = value + far[index, j - 1].astype(jnp.float32)
-        out[index] = value.astype(jnp.bfloat16)
+
+        @pl.when(far_end)
+        def _():
+            collect(z_index)
+
+        collect(index)
     else:
+        take_extra()
         drain(2, 5, True, total)
-        run(final, 2, 4, 0, pieces)
-        stage(0, final, 2, 4)
-        stage(1, final, 2, 4)
+        run(final, 0, 4, 0, pieces)
+        stage(0, final, 0, 4)
+        stage(1, final, 0, 4)
         finish_all()
         stage(2, final - 1)
         stage(2, final, 0, 4)
@@ -495,7 +526,7 @@
             pltpu.VMEM((width // piece, count_rows, piece), jnp.float32),
             pltpu.VMEM((width // piece, count_rows, piece), jnp.bfloat16),
             pltpu.VMEM((5, count_rows, block), jnp.float32),
-            pltpu.VMEM((block // rows, count_rows, rows), jnp.float32),
+            pltpu.VMEM((2, block // rows, count_rows, rows), jnp.float32),
             pltpu.VMEM((total, tp, share, block), jnp.bfloat16),
             pltpu.VMEM((total, tp - 1, share, block), jnp.bfloat16),
             dma((min(SLOTS, 4 * count),)),

time: 455 us -> 449 us (0.987)
  Pallas kernels: 454 us -> 449 us
    pallas_call x1, Pallas kernels: 437 us -> 431 us  [gather(): pl.pallas_call(functools.partial(gather_kernel, (n, tp, local, block, row...]
where the time goes in v6:
time: 449 us
  Pallas kernels  449 us (100%)
    pallas_call x1, Pallas kernels, gather(): pl.pallas_call(functools.partial(gather_kernel, (n, tp, local, block, row...  431 us
    pallas_call x1, Pallas kernels, per_device(): pl.pallas_call(functools.partial(write_kernel, parts), out_shape=[weight,...  17.2 us

profile of v6, /device:TPU:0, one launch (start us, length us, event | category | flops | bytes accessed | tf_op | source)
XLA Modules:
  0.0 449.3 jit_solution(11959076275410553428)
XLA Ops:
  0.6 431.5 %gather_both.1 = (bf16[2,3584,3584]{2,1,0:T(8,128)(2,1)S(1)}, bf16[16,32,224]{2,1,0:T(8,128)(2,1)S(1)}) custom-call(bf16[128,3584]{1,0:T(8,128)(2,1)} %tokens.1, f32[7,128]{1,0:T(8,128)} %bitcast.1, f32[896,3584]{1,0:T(8,128)} %up.1, f32[896,3584]{1,0:T(8,128)} %down.1), custom_call_target="tpu_custom_call" | custom-call | bytes 57802752 | tf_op jit(solution)/shard_map/gather_both/pallas_call | solution.py:513
  432.1 17.2 %write_out.1 = (bf16[3584,3584]{1,0:T(8,128)(2,1)}, bf16[3584,3584]{1,0:T(8,128)(2,1)}, bf16[32,3584]{1,0:T(8,128)(2,1)}) custom-call(bf16[2,3584,3584]{2,1,0:T(8,128)(2,1)S(1)} %get-tuple-element.5.both, bf16[16,32,224]{2,1,0:T(8,128)(2,1)S(1)} %get-tuple-element.6.mixed), custom_call_target="tpu_custom_call" | custom-call | tf_op jit(solution)/shard_map/write_out/pallas_call | solution.py:575

commit v7 on v6

--- a/solution.py
+++ b/solution.py
@@ -9,7 +9,7 @@
 
 MESH = pl.DeviceIdType.MESH
 SLOTS = 6
-LAG = 2
+LAG = 1
 
 
 def divisor(total, most, least):
@@ -463,7 +463,6 @@
 
         drain(2, 5, True, total - 1)
         rest(total - 1, 2, 5, True)
-        stage(2, final - 1)
         _, source, _ = x_of(total - 1)
         index = source * every + other * blocks + blocks - 1
         fill(0, index, 0, per_block - 1)
@@ -473,6 +472,7 @@
         fill(0, index, per_block - 1, per_block)
         share_all(index)
         finish_all()
+        stage(2, final - 1)
 
         @pl.when(far_end)
         def _():

time: 449 us -> 449 us (level)
  no operation moved by 1% of the time
where the time goes in v7:
time: 449 us
  Pallas kernels  448 us (100%)
    pallas_call x1, Pallas kernels, gather(): pl.pallas_call(functools.partial(gather_kernel, (n, tp, local, block, row...  431 us
    pallas_call x1, Pallas kernels, per_device(): pl.pallas_call(functools.partial(write_kernel, parts), out_shape=[weight,...  17.2 us

profile of v7, /device:TPU:0, one launch (start us, length us, event | category | flops | bytes accessed | tf_op | source)
XLA Modules:
  0.0 448.8 jit_solution(17875875263324978203)
XLA Ops:
  0.6 431.0 %gather_both.1 = (bf16[2,3584,3584]{2,1,0:T(8,128)(2,1)S(1)}, bf16[16,32,224]{2,1,0:T(8,128)(2,1)S(1)}) custom-call(bf16[128,3584]{1,0:T(8,128)(2,1)} %tokens.1, f32[7,128]{1,0:T(8,128)} %bitcast.1, f32[896,3584]{1,0:T(8,128)} %up.1, f32[896,3584]{1,0:T(8,128)} %down.1), custom_call_target="tpu_custom_call" | custom-call | bytes 57802752 | tf_op jit(solution)/shard_map/gather_both/pallas_call | solution.py:513
  431.6 17.2 %write_out.1 = (bf16[3584,3584]{1,0:T(8,128)(2,1)}, bf16[3584,3584]{1,0:T(8,128)(2,1)}, bf16[32,3584]{1,0:T(8,128)(2,1)}) custom-call(bf16[2,3584,3584]{2,1,0:T(8,128)(2,1)S(1)} %get-tuple-element.5.both, bf16[16,32,224]{2,1,0:T(8,128)(2,1)S(1)} %get-tuple-element.6.mixed), custom_call_target="tpu_custom_call" | custom-call | tf_op jit(solution)/shard_map/write_out/pallas_call | solution.py:575

commit v8 on v7

--- a/solution.py
+++ b/solution.py
@@ -154,9 +154,7 @@
             def _(way=way):
                 along(way, m, 0, q).start()
 
-    lax.fori_loop(0, slots, lambda i, c: (next_load(i), c)[1], 0)
-    token_copy = pltpu.make_async_copy(tokens, held, token_s.at[0])
-    token_copy.start()
+    start_load(0, g, 0, 0)
 
     barrier = pltpu.get_barrier_semaphore()
     for way in range(2):
@@ -170,6 +168,9 @@
 
     for j in range(1, tp):
         pl.semaphore_signal(barrier, inc=1, device_id=(g, f, mate(j)), device_id_type=MESH)
+    lax.fori_loop(1, slots, lambda i, c: (next_load(i), c)[1], 0)
+    token_copy = pltpu.make_async_copy(tokens, held, token_s.at[0])
+    token_copy.start()
     step_rows = divisor(local, 128, 8)
     eye = lax.broadcasted_iota(jnp.int32, (step_rows, step_rows), 0) == lax.broadcasted_iota(
         jnp.int32, (step_rows, step_rows), 1)

time: 449 us -> 449 us (level)
  no operation moved by 1% of the time
where the time goes in v8:
time: 449 us
  Pallas kernels  448 us (100%)
    pallas_call x1, Pallas kernels, gather(): pl.pallas_call(functools.partial(gather_kernel, (n, tp, local, block, row...  431 us
    pallas_call x1, Pallas kernels, per_device(): pl.pallas_call(functools.partial(write_kernel, parts), out_shape=[weight,...  17.2 us

profile of v8, /device:TPU:0, one launch (start us, length us, event | category | flops | bytes accessed | tf_op | source)
XLA Modules:
  0.0 448.8 jit_solution(2994613627465646015)
XLA Ops:
  0.6 431.0 %gather_both.1 = (bf16[2,3584,3584]{2,1,0:T(8,128)(2,1)S(1)}, bf16[16,32,224]{2,1,0:T(8,128)(2,1)S(1)}) custom-call(bf16[128,3584]{1,0:T(8,128)(2,1)} %tokens.1, f32[7,128]{1,0:T(8,128)} %bitcast.1, f32[896,3584]{1,0:T(8,128)} %up.1, f32[896,3584]{1,0:T(8,128)} %down.1), custom_call_target="tpu_custom_call" | custom-call | bytes 57802752 | tf_op jit(solution)/shard_map/gather_both/pallas_call | solution.py:514
  431.6 17.2 %write_out.1 = (bf16[3584,3584]{1,0:T(8,128)(2,1)}, bf16[3584,3584]{1,0:T(8,128)(2,1)}, bf16[32,3584]{1,0:T(8,128)(2,1)}) custom-call(bf16[2,3584,3584]{2,1,0:T(8,128)(2,1)S(1)} %get-tuple-element.5.both, bf16[16,32,224]{2,1,0:T(8,128)(2,1)S(1)} %get-tuple-element.6.mixed), custom_call_target="tpu_custom_call" | custom-call | tf_op jit(solution)/shard_map/write_out/pallas_call | solution.py:576
